TPU v7x, 32 devices: a whole 2x2x4 slice. The times are simulated.
32 devices in a mesh: sp: 8 (over z, y), tp: 4 (over x, core).
Axes of the slice: x: 2, y: 2, z: 4, core: 2. Of those that a mesh axis runs over, the one named last changes fastest.
Arguments:
- stream_in: bfloat16 [6144, 2048], P(('sp', 'tp')), may hold values from -6 to 6
- query_wide: bfloat16 [6144, 512], P('sp', 'tp'), may hold values from -6 to 6
- key_wide: bfloat16 [6144, 512], P('sp', 'tp'), may hold values from -6 to 6
- value_wide: bfloat16 [6144, 512], P('sp', 'tp'), may hold values from -6 to 6
- gate_wide: bfloat16 [6144, 512], P('sp', 'tp'), may hold values from -6 to 6
- decay_wide: float32 [4, 6144], P('tp', 'sp'), may hold values from -2.3 to 0, as said below
- query_narrow: bfloat16 [6144, 512], P('sp', 'tp'), may hold values from -6 to 6
- key_narrow: bfloat16 [6144, 512], P('sp', 'tp'), may hold values from -6 to 6
- value_narrow: bfloat16 [6144, 512], P('sp', 'tp'), may hold values from -6 to 6
- gate_narrow: bfloat16 [6144, 512], P('sp', 'tp'), may hold values from -6 to 6
- decay_narrow: float32 [8, 6144], P('tp', 'sp'), may hold values from -2.3 to 0, as said below
- output_wide: bfloat16 [512, 2048], P('tp'), may hold values from -0.25 to 0.25
- output_narrow: bfloat16 [512, 2048], P('tp'), may hold values from -0.25 to 0.25
- norm_gain: bfloat16 [2048], replicated, may hold values from 0.099609375 to 1.8984375
- up_weight: bfloat16 [2048, 8192], P('sp', 'tp'), may hold values from -0.125 to 0.125
- down_weight: bfloat16 [8192, 2048], P('tp', 'sp'), may hold values from -0.0625 to 0.0625
Outputs:
- layer_out: bfloat16 [6144, 2048], P(('sp', 'tp'))
Inputs may be any that keep to these rules, and one draw needn't show every extreme that they name: `decay_wide`: each entry is the logarithm of one head's retention factor at one position. `decay_narrow`: each entry is the logarithm of one head's retention factor at one position.
All inputs are finite; a program needn't handle non-finite values.
Results may differ from a plain program's by a relative error of at most 0.02.
Values may be sent and summed in bfloat16 or wider, within the bound.
A program may use at most 128 MiB of HBM per device.

v0:
```python
import functools
import jax
import jax.numpy as jnp
import numpy as np
from jax import lax
from jax.experimental import pallas as pl
from jax.experimental.pallas import tpu as pltpu
from jax.sharding import PartitionSpec as P

HDW = 128
HDN = 64
BLOCK = 128


head_eps = 1e-05
norm_eps = 1e-06
rope_base = 10000.0


def carried_in(shard, axis, join, neutral):
    place = lax.axis_index(axis)
    gathered = jax.tree.map(
        lambda a, kind: lax.all_gather(a.astype(kind), axis),
        shard,
        (jnp.bfloat16, jnp.bfloat16, jnp.bfloat16, jnp.bfloat16),
    )
    state = jax.tree.map(lambda a, e: jnp.zeros_like(a) + jnp.asarray(e, a.dtype), shard, neutral)

    def one(turn, state):
        return join(
            state,
            jax.tree.map(
                lambda a, own: lax.dynamic_index_in_dim(a, turn, 0, False).astype(own.dtype),
                gathered,
                shard,
            ),
        )

    return lax.fori_loop(0, place, one, state)


def rotate(values, places):
    half = values.shape[-1] // 2
    inverse = rope_base ** (-jnp.arange(half, dtype=jnp.float32) / half)
    angles = places[:, None] * inverse[None, :]
    cosine = jnp.cos(angles)[:, None, :]
    sine = jnp.sin(angles)[:, None, :]
    front = values[..., :half]
    back = values[..., half:]
    return jnp.concatenate([front * cosine - back * sine, back * cosine + front * sine], axis=-1)


def block_step(carried, inputs):
    query, keys, values, log_rate = inputs
    running = jnp.cumsum(log_rate, axis=0)
    spread = running[:, None, :] - running[None, :, :]
    length = log_rate.shape[0]
    lower = (jnp.arange(length)[:, None] >= jnp.arange(length)[None, :])[:, :, None]
    factor = jnp.where(lower, jnp.exp(jnp.minimum(spread, 0.0)), 0.0)
    scores = jnp.einsum("thd,shd->tsh", query, keys) * factor
    within = jnp.einsum("tsh,she->the", scores, values)
    across = jnp.einsum("thd,hde->the", query, carried) * jnp.exp(running)[:, :, None]
    tail_decay = jnp.exp(running[-1][None, :] - running)
    updated = jnp.exp(running[-1])[:, None, None] * carried + jnp.einsum(
        "shd,she->hde", keys * tail_decay[:, :, None], values
    )
    return (updated, within + across)


def head_norm(values):
    centre = values - jnp.mean(values, axis=-1, keepdims=True)
    spread = jnp.mean(centre * centre, axis=-1, keepdims=True)
    return centre * lax.rsqrt(spread + head_eps)


def local_group(query, keys, values, log_rate, width, places):
    length = query.shape[0]
    count_of_heads = query.shape[1] // width
    blocks = length // BLOCK

    def split(array):
        return array.astype(jnp.float32).reshape(length, count_of_heads, width)

    query_rot = rotate(split(query), places)
    keys_rot = rotate(split(keys), places) * width ** (-0.5)
    rates = log_rate.T
    carried = jnp.zeros((count_of_heads, width, width), jnp.float32)
    final_state, outputs = lax.scan(
        block_step,
        carried,
        (
            query_rot.reshape(blocks, BLOCK, count_of_heads, width),
            keys_rot.reshape(blocks, BLOCK, count_of_heads, width),
            split(values).reshape(blocks, BLOCK, count_of_heads, width),
            rates.reshape(blocks, BLOCK, count_of_heads),
        ),
    )
    running = jnp.cumsum(rates, axis=0)
    return (
        query_rot,
        outputs.reshape(length, count_of_heads, width),
        final_state,
        jnp.exp(running[-1]),
        running,
    )


def finish_group(query_rot, outputs, incoming, running, gate):
    length = outputs.shape[0]
    outputs = (
        outputs + jnp.einsum("thd,hde->the", query_rot, incoming) * jnp.exp(running)[:, :, None]
    )
    normed = head_norm(outputs).reshape(length, -1)
    return (jax.nn.silu(gate.astype(jnp.float32)) * normed).astype(jnp.bfloat16)


def chain(earlier, later):
    rate_wide, memory_wide, rate_narrow, memory_narrow = earlier
    later_rate_wide, later_memory_wide, later_rate_narrow, later_memory_narrow = later
    return (
        rate_wide * later_rate_wide,
        memory_wide * later_rate_wide[:, None, None] + later_memory_wide,
        rate_narrow * later_rate_narrow,
        memory_narrow * later_rate_narrow[:, None, None] + later_memory_narrow,
    )


def row_norm(middle, norm_gain):
    middle_f = middle.astype(jnp.float32)
    scale = lax.rsqrt(jnp.mean(middle_f * middle_f, axis=-1, keepdims=True) + norm_eps)
    return (middle_f * scale * norm_gain.astype(jnp.float32)).astype(jnp.bfloat16)


def on_device(
    stream_in,
    query_wide,
    key_wide,
    value_wide,
    gate_wide,
    decay_wide,
    query_narrow,
    key_narrow,
    value_narrow,
    gate_narrow,
    decay_narrow,
    output_wide,
    output_narrow,
    norm_gain,
    up_weight,
    down_weight,
):
    length = query_wide.shape[0]
    places = (lax.axis_index("sp") * length + jnp.arange(length, dtype=jnp.int32)).astype(
        jnp.float32
    )
    wide_query, wide_out, wide_state, wide_total, wide_running = local_group(
        query_wide, key_wide, value_wide, decay_wide, HDW, places
    )
    narrow_query, narrow_out, narrow_state, narrow_total, narrow_running = local_group(
        query_narrow, key_narrow, value_narrow, decay_narrow, HDN, places
    )
    identity = (
        jnp.ones_like(wide_total),
        jnp.zeros_like(wide_state),
        jnp.ones_like(narrow_total),
        jnp.zeros_like(narrow_state),
    )
    incoming = carried_in(
        (wide_total, wide_state, narrow_total, narrow_state), "sp", chain, identity
    )
    mixed_wide = finish_group(wide_query, wide_out, incoming[1], wide_running, gate_wide)
    mixed_narrow = finish_group(narrow_query, narrow_out, incoming[3], narrow_running, gate_narrow)
    mixed_sum = lax.psum_scatter(
        (
            jnp.dot(mixed_wide, output_wide, preferred_element_type=jnp.float32)
            + jnp.dot(mixed_narrow, output_narrow, preferred_element_type=jnp.float32)
        ).astype(jnp.bfloat16),
        "tp",
        scatter_dimension=0,
        tiled=True,
    ).astype(jnp.float32)
    middle = (stream_in.astype(jnp.float32) + mixed_sum).astype(jnp.bfloat16)
    normed = lax.all_gather(row_norm(middle, norm_gain), "tp", axis=0, tiled=True)
    up_sum = jnp.dot(
        normed,
        lax.all_gather(up_weight, "sp", axis=0, tiled=True),
        preferred_element_type=jnp.float32,
    )
    hidden = jnp.square(jax.nn.relu(up_sum)).astype(jnp.bfloat16)
    down_sum = jnp.dot(
        hidden,
        lax.all_gather(down_weight, "sp", axis=1, tiled=True),
        preferred_element_type=jnp.float32,
    )
    down_rows = lax.psum_scatter(
        down_sum.astype(jnp.bfloat16), "tp", scatter_dimension=0, tiled=True
    ).astype(jnp.float32)
    return (middle.astype(jnp.float32) + down_rows).astype(jnp.bfloat16)


F32 = jnp.float32
BF16 = jnp.bfloat16
MESH_ID = pl.DeviceIdType.MESH


def turn_tables(shards, length):
    lane = np.arange(128)
    offsets, starts = [], []
    for width in (HDW, HDN):
        half = width // 2
        inverse = rope_base ** (-((lane % half).astype(np.float64)) / half)
        inside = np.arange(BLOCK)[:, None] * inverse[None, :]
        first = (np.arange(shards * length // BLOCK) * BLOCK)[:, None] * inverse[None, :]
        offsets += [np.cos(inside), np.sin(inside)]
        starts += [np.cos(first), np.sin(first)]
    return np.stack(offsets).astype(np.float32), np.stack(starts).astype(np.float32)


def dot(a, b):
    return jnp.dot(a, b, preferred_element_type=F32)


def dot_rows(a, b):
    return lax.dot_general(a, b, (((0,), (0,)), ((), ())), preferred_element_type=F32)


def dot_cols(a, b):
    return lax.dot_general(a, b, (((1,), (1,)), ((), ())), preferred_element_type=F32)


def layer_kernel(
    SP, TP,
    stream, qw, kw, vw, gw, qn, kn, vn, gn, decay, offs, starts, gain, ow_w, ow_n, up, down,
    out,
    up_buf, down_buf, ow_buf, st_in, k_rot, before, inside, mixed, mix_in, mid, rows, hidden, part, part_in,
    ssem, rsem, lsem, zsend, zrecv,
):
    sp = lax.axis_index("sp")
    tp = lax.axis_index("tp")
    NZ = SP // 2
    z = sp // 2
    y = sp % 2
    T = qw.shape[0]
    NB = T // BLOCK
    RT = T // TP
    RB = up.shape[0]
    CB = down.shape[1]
    D = stream.shape[1]
    FH = up.shape[1] // 2
    mate = tp + 1 - 2 * (tp % 2)

    def at(dz, dy):
        return ((z + dz) % NZ) * 2 + (y + dy) % 2

    count = [0]
    pending = []

    def send(src, dst, device):
        k = count[0]
        count[0] += 1
        copy = pltpu.make_async_remote_copy(
            src_ref=src, dst_ref=dst, send_sem=ssem.at[k], recv_sem=rsem.at[k],
            device_id=device, device_id_type=MESH_ID,
        )
        copy.start()
        pending.append(copy)
        return copy

    def group(dy, dt):
        return (z * 2 + (y + dy) % 2, (tp + dt) % TP)

    def to_sp(i):
        return (i, tp)

    def to_tp(i):
        return (sp, i)

    barrier = pltpu.get_barrier_semaphore()
    for d in range(1, SP):
        pl.semaphore_signal(barrier, inc=1, device_id=to_sp((sp + d) % SP), device_id_type=MESH_ID)
    for d in range(1, TP):
        pl.semaphore_signal(barrier, inc=1, device_id=to_tp((tp + d) % TP), device_id_type=MESH_ID)
    for d in range(1, TP):
        pl.semaphore_signal(barrier, inc=1, device_id=group(1, d), device_id_type=MESH_ID)
    pl.semaphore_wait(barrier, SP + 2 * TP - 3)

    def up_at(i):
        return up_buf.at[pl.ds(pl.multiple_of(i * RB, RB), RB), :]

    def down_at(i):
        return down_buf.at[i]

    place = (up_at, down_at)

    def hidden_half(w, half):
        cut = pl.ds(pl.multiple_of(half * FH, FH), FH)
        return up.at[:, cut] if w == 0 else down.at[cut, :]

    across_y = to_sp(at(0, 1))
    line_waits = []

    def piece(w, dy, zs):
        return place[w](zs * 2 + (y + dy) % 2)

    def line_copy(w, dy, zs, src, slot, device_z):
        return pltpu.make_async_remote_copy(
            src_ref=src, dst_ref=piece(w, dy, zs), send_sem=zsend.at[slot],
            recv_sem=zrecv.at[(w * 2 + dy) * NZ + zs],
            device_id=to_sp(device_z * 2 + y), device_id_type=MESH_ID,
        )

    def line_start(when, copy):
        @pl.when(when)
        def _():
            copy.start()

        line_waits.append((when, copy))

    def line_send(w, dy):
        for t in (1, 2, 0, 3):
            src = hidden_half(w, y) if dy == 0 else piece(w, dy, z)
            far = ((z == 0) & (t == 3)) | ((z == NZ - 1) & (t == 0))
            line_start((z != t) & jnp.logical_not(far), line_copy(w, dy, z, src, (w * 2 + dy) * 5 + t, t))

    def line_wait(w, dy, zs):
        line_copy(w, dy, zs, piece(w, dy, zs), 0, (z + 1) % NZ).wait_recv()

    def line_relay(w, dy):
        for me, source, target in ((2, 0, 3), (1, 3, 0)):
            @pl.when(z == me)
            def _():
                line_wait(w, dy, source)

            slot = (w * 2 + dy) * 5 + 4
            line_start(z == me, line_copy(w, dy, source, piece(w, dy, source), slot, target))

    def line_arrived(w, dy, d):
        zs = (z + d * (1 + 2 * (z // 2))) % NZ
        relayed = ((z == 2) & (zs == 0)) | ((z == 1) & (zs == 3))

        @pl.when(jnp.logical_not(relayed))
        def _():
            line_wait(w, dy, zs)

        return zs * 2 + (y + dy) % 2

    up_y = send(hidden_half(0, (y + 1) % 2), up_at(sp), across_y)
    line_send(0, 0)

    locals_ = []

    def keep(src, dst):
        copy = pltpu.make_async_copy(src, dst, lsem.at[len(locals_)])
        copy.start()
        locals_.append(copy)

    def ow_at(i, g):
        return ow_buf.at[i, pl.ds(g * 128, 128), :]

    ow_mate = [send(r, ow_at(tp, g), to_tp(mate)) for g, r in enumerate((ow_w, ow_n))]
    ow_far = [
        (q, g, send(r, ow_at(tp, g), to_tp((tp + 2 * q) % TP)))
        for q in range(1, TP // 2) for g, r in enumerate((ow_w, ow_n))
    ]
    keep(hidden_half(0, y), up_at(sp))
    keep(hidden_half(1, y), down_at(sp))
    keep(ow_w, ow_at(tp, 0))
    keep(ow_n, ow_at(tp, 1))

    lane = lax.broadcasted_iota(jnp.int32, (128, 128), 1)
    row = lax.broadcasted_iota(jnp.int32, (128, 128), 0)
    lower = row >= lane
    low = lane < HDN
    low_row = row < HDN
    diagonal = low == low_row
    cr = decay[...]
    step = 1
    while step < 128:
        cr = cr + jnp.where(lane >= step, pltpu.roll(cr, step, 1), 0.0)
        step *= 2
    ct = cr.T

    def col(h, b):
        return ct[:, h * NB + b:h * NB + b + 1]

    def line(h, b):
        return cr[h * NB + b:h * NB + b + 1, :]

    def total(h, b):
        return cr[h * NB + b:h * NB + b + 1, 127:128]

    def pair(a, b):
        return jnp.where(low, a, b)

    sign_w = jnp.where(low, -1.0, 1.0)
    early = (lane % HDN) < HDN // 2
    sign_n = jnp.where(early, -1.0, 1.0)

    def tables(g, b):
        cb = starts[2 * g, pl.ds(sp * NB + b, 1), :]
        sb = starts[2 * g + 1, pl.ds(sp * NB + b, 1), :]
        co, so = offs[2 * g], offs[2 * g + 1]
        return co * cb - so * sb, (so * cb + co * sb) * (sign_n if g else sign_w)

    def turned(x, table, g):
        if g:
            other = jnp.where(early, pltpu.roll(x, 128 - HDN // 2, 1), pltpu.roll(x, HDN // 2, 1))
        else:
            other = pltpu.roll(x, HDW // 2, 1)
        return x * table[0] + other * table[1]

    state_w = jnp.zeros((128, 128), F32)
    state_n = jnp.zeros((128, 128), F32)
    sums = [jnp.zeros((1, 1), F32) for _ in range(3)]
    for b in range(NB):
        rs = pl.ds(b * BLOCK, BLOCK)
        before[0, b] = state_w
        before[1, b] = state_n
        kwr = turned(kw[rs, :].astype(F32), tables(0, b), 0) * HDW ** (-0.5)
        knr = turned(kn[rs, :].astype(F32), tables(1, b), 1) * HDN ** (-0.5)
        k_rot[rs, 0:128] = kwr.astype(BF16)
        k_rot[rs, 128:256] = knr.astype(BF16)
        t0, t1, t2 = total(0, b), total(1, b), total(2, b)
        sums = [s + t for s, t in zip(sums, (t0, t1, t2))]
        tail_w = jnp.exp(t0 - col(0, b))
        tail_n = pair(jnp.exp(t1 - col(1, b)), jnp.exp(t2 - col(2, b)))
        state_w = jnp.exp(t0) * state_w + dot_rows((kwr * tail_w).astype(BF16), vw[rs, :])
        grown = dot_rows((knr * tail_n).astype(BF16), vn[rs, :])
        state_n = jnp.where(low_row, jnp.exp(t1), jnp.exp(t2)) * state_n + jnp.where(diagonal, grown, 0.0)
    small = lax.broadcasted_iota(jnp.int32, (16, 128), 0)
    rates = jnp.where(small == 0, jnp.exp(sums[0]), jnp.where(small == 1, jnp.exp(sums[1]), jnp.exp(sums[2])))
    st_in[sp, 0:128, :] = state_w.astype(BF16)
    st_in[sp, 128:256, :] = state_n.astype(BF16)
    st_in[sp, 256:272, :] = rates.astype(BF16)
    states = [send(st_in.at[sp], st_in.at[sp], to_sp((sp + d) % SP)) for d in range(1, SP)]

    for b in range(NB):
        rs = pl.ds(b * BLOCK, BLOCK)
        kwr, knr = k_rot[rs, 0:128], k_rot[rs, 128:256]
        qwr = turned(qw[rs, :].astype(F32), tables(0, b), 0)
        qnr = turned(qn[rs, :].astype(F32), tables(1, b), 1)

        def factor(h):
            return jnp.where(lower, jnp.exp(jnp.minimum(col(h, b) - line(h, b), 0.0)), 0.0)

        scores = (dot_cols(qwr.astype(BF16), kwr) * factor(0)).astype(BF16)
        inside[rs, 0:128] = dot(scores, vw[rs, :])
        near = (dot_cols(jnp.where(low, qnr, 0.0).astype(BF16), knr) * factor(1)).astype(BF16)
        far = (dot_cols(jnp.where(low, 0.0, qnr).astype(BF16), knr) * factor(2)).astype(BF16)
        inside[rs, 128:256] = pair(dot(near, vn[rs, :]), dot(far, vn[rs, :]))
        k_rot[rs, 0:128] = (qwr * jnp.exp(col(0, b))).astype(BF16)
        k_rot[rs, 128:256] = (qnr * pair(jnp.exp(col(1, b)), jnp.exp(col(2, b)))).astype(BF16)

    up_y.wait_recv()
    line_send(0, 1)
    down_y = send(hidden_half(1, (y + 1) % 2), down_at(sp), across_y)
    line_send(1, 0)

    for copy in states:
        copy.wait_recv()
    s_w = jnp.zeros((128, 128), F32)
    s_n = jnp.zeros((128, 128), F32)
    for j in range(SP):
        r = st_in[j, 256:272, :].astype(F32)
        s_w = jnp.where(j < sp, s_w * r[0:1, :] + st_in[j, 0:128, :].astype(F32), s_w)
        s_n = jnp.where(
            j < sp, s_n * jnp.where(low_row, r[1:2, :], r[2:3, :]) + st_in[j, 128:256, :].astype(F32), s_n
        )

    sums = [jnp.zeros((1, 1), F32) for _ in range(3)]
    for b in range(NB):
        rs = pl.ds(b * BLOCK, BLOCK)
        whole_w = before[0, b] + jnp.exp(sums[0]) * s_w
        whole_n = before[1, b] + jnp.where(low_row, jnp.exp(sums[1]), jnp.exp(sums[2])) * s_n
        sums = [s + total(h, b) for h, s in enumerate(sums)]
        o_w = inside[rs, 0:128] + dot(k_rot[rs, 0:128], whole_w.astype(BF16))
        o_n = inside[rs, 128:256] + dot(k_rot[rs, 128:256], whole_n.astype(BF16))

        def both(x):
            first = jnp.sum(jnp.where(low, x, 0.0), axis=-1, keepdims=True) / HDN
            second = jnp.sum(jnp.where(low, 0.0, x), axis=-1, keepdims=True) / HDN
            return pair(first, second)

        c_w = o_w - jnp.mean(o_w, axis=-1, keepdims=True)
        n_w = c_w * lax.rsqrt(jnp.mean(c_w * c_w, axis=-1, keepdims=True) + head_eps)
        c_n = o_n - both(o_n)
        n_n = c_n * lax.rsqrt(both(c_n * c_n) + head_eps)
        mixed[rs, 0:128] = (jax.nn.silu(gw[rs, :].astype(F32)) * n_w).astype(BF16)
        mixed[rs, 128:256] = (jax.nn.silu(gn[rs, :].astype(F32)) * n_n).astype(BF16)

    def my_rows(i):
        return pl.ds(pl.multiple_of(i * RT, RT), RT)

    swaps = [
        send(mixed.at[my_rows((tp + d) % TP), :], mix_in.at[tp], to_tp((tp + d) % TP)) for d in range(1, TP)
    ]
    mix_in[tp] = mixed[my_rows(tp), :]
    ow_relay = []
    for q, g, copy in ow_far:
        copy.wait_recv()
        came = (tp + TP - 2 * q) % TP
        ow_relay.append(send(ow_at(came, g), ow_at(came, g), to_tp(mate)))
    line_relay(0, 0)
    for copy in swaps + ow_mate + ow_relay:
        copy.wait_recv()
    for copy in locals_:
        copy.wait()

    def project(c, _):
        cs = pl.ds(pl.multiple_of(c * 512, 512), 512)
        acc = stream[:, cs].astype(F32)
        for i in range(TP):
            acc = acc + dot(mix_in[i], ow_buf[i, :, cs])
        mid[:, cs] = acc.astype(BF16)
        return 0

    lax.fori_loop(0, D // 512, project, 0)

    def norm(i, _):
        m = mid[pl.ds(pl.multiple_of(i * 32, 32), 32), :].astype(F32)
        scale = lax.rsqrt(jnp.mean(m * m, axis=-1, keepdims=True) + norm_eps)
        rows[pl.ds(pl.multiple_of((y * TP + tp) * RT + i * 32, 32), 32), :] = (m * scale * gain[...].astype(F32)).astype(BF16)
        return 0

    lax.fori_loop(0, RT // 32, norm, 0)

    def block(dy, dt):
        return rows.at[my_rows((y + dy) % 2 * TP + (tp + dt) % TP), :]

    near_x = send(block(0, 0), block(0, 0), group(0, 2))
    near_y = send(block(0, 0), block(0, 0), group(1, 0))
    hand = [send(block(0, 0), block(0, 0), to_tp(mate))]
    line_relay(0, 1)
    down_y.wait_recv()
    line_send(1, 1)
    near_x.wait_recv()
    corner = send(block(0, 2), block(0, 2), group(1, 0))
    hand.append(send(block(0, 2), block(0, 2), to_tp(mate)))
    near_y.wait_recv()
    hand.append(send(block(1, 0), block(1, 0), to_tp(mate)))
    for dy in range(2):
        for d in range(1, NZ):
            line_arrived(0, dy, d)

    def up_rows(dy, dp):
        i = (y + dy) % 2 * (TP // 2) + (tp // 2 + dp) % (TP // 2)
        rs = pl.ds(pl.multiple_of(i * 2 * RT, 2 * RT), 2 * RT)

        def one(c, _):
            cs = pl.ds(pl.multiple_of(c * 512, 512), 512)
            h = jnp.maximum(dot(rows[rs, :], up_buf[:, cs]), 0.0)
            hidden[rs, cs] = (h * h).astype(BF16)
            return 0

        lax.fori_loop(0, FH // 512, one, 0)

    hand[0].wait_recv()
    up_rows(0, 0)
    corner.wait_recv()
    hand.append(send(block(1, 2), block(1, 2), to_tp(mate)))
    line_relay(1, 0)
    hand[1].wait_recv()
    up_rows(0, 1)
    hand[2].wait_recv()
    up_rows(1, 0)
    hand[3].wait_recv()
    up_rows(1, 1)

    peers = [(dy, dt) for dy in range(2) for dt in range(TP) if dy or dt]

    def chunk(k, j):
        def one(i, _):
            rs = pl.ds(pl.multiple_of(i * 2 * RT, 2 * RT), 2 * RT)
            part[k, rs, :] = dot(hidden[rs, :], down_buf[j]).astype(BF16)
            return 0

        lax.fori_loop(0, TP, one, 0)
        return [
            send(
                part.at[k, my_rows((y + dy) % 2 * TP + (tp + dt) % TP), :],
                part_in.at[k, dy * TP + dt - 1], group(dy, dt),
            )
            for dy, dt in peers
        ]

    def finish(k, j, copies):
        for copy in copies:
            copy.wait_recv()
        cs = pl.ds(pl.multiple_of(j * CB, CB), CB)
        acc = mid[:, cs].astype(F32) + part[k, my_rows(y * TP + tp), :].astype(F32)
        for d in range(2 * TP - 1):
            acc = acc + part_in[k, d].astype(F32)
        out[:, cs] = acc.astype(BF16)

    done = []
    for k in range(SP):
        d, dy = k // 2, (y + k) % 2
        if k == 4:
            line_relay(1, 1)
        j = line_arrived(1, dy, d) if d else at(0, dy)
        done.append((k, j, chunk(k, j)))
        if k > 1:
            finish(*done[k - 2])
    finish(*done[-2])
    finish(*done[-1])
    for when, copy in line_waits:
        @pl.when(when)
        def _(copy=copy):
            copy.wait_send()
    for copy in pending:
        copy.wait_send()


def one_kernel(SP, TP, *args):
    (stream, qw, kw, vw, gw, dw, qn, kn, vn, gn, dn, ow, on, gain, up, down) = args
    T = qw.shape[0]
    NB = T // BLOCK
    D = stream.shape[1]
    RT = T // TP
    FH = up.shape[1] // 2
    CB = down.shape[1]
    heads = dw.shape[0] + dn.shape[0]
    decay = jnp.concatenate([dw, dn]).reshape(heads * NB, BLOCK)
    decay = jnp.pad(decay, ((0, 128 - heads * NB), (0, 0)))
    offs, starts = turn_tables(SP, T)
    vmem = pl.BlockSpec(memory_space=pltpu.VMEM)
    hbm = pl.BlockSpec(memory_space=pl.ANY)
    copies = 96
    return pl.pallas_call(
        functools.partial(layer_kernel, SP, TP),
        out_shape=jax.ShapeDtypeStruct((RT, D), BF16),
        in_specs=[vmem] * 13 + [hbm] * 4,
        out_specs=vmem,
        scratch_shapes=[
            pltpu.VMEM((D, FH), BF16),
            pltpu.VMEM((SP, FH, CB), BF16),
            pltpu.VMEM((TP, 256, D), BF16),
            pltpu.VMEM((SP, 272, 128), BF16),
            pltpu.VMEM((T, 256), BF16),
            pltpu.VMEM((2, NB, 128, 128), F32),
            pltpu.VMEM((T, 256), F32),
            pltpu.VMEM((T, 256), BF16),
            pltpu.VMEM((TP, RT, 256), BF16),
            pltpu.VMEM((RT, D), BF16),
            pltpu.VMEM((2 * T, D), BF16),
            pltpu.VMEM((2 * T, FH), BF16),
            pltpu.VMEM((SP, 2 * T, CB), BF16),
            pltpu.VMEM((SP, 2 * TP - 1, RT, CB), BF16),
            pltpu.SemaphoreType.DMA((copies,)),
            pltpu.SemaphoreType.DMA((copies,)),
            pltpu.SemaphoreType.DMA((4,)),
            pltpu.SemaphoreType.DMA((20,)),
            pltpu.SemaphoreType.DMA((2 * SP,)),
        ],
        compiler_params=pltpu.CompilerParams(
            collective_id=0, has_side_effects=True, vmem_limit_bytes=60 * 1024 * 1024
        ),
    )(stream, qw, kw, vw, gw, qn, kn, vn, gn, decay, jnp.asarray(offs), jnp.asarray(starts),
      gain.reshape(1, D), ow, on, up, down)


def fits_kernel(SP, TP, args):
    D, FF = args[14].shape
    T = args[1].shape[0] // SP
    return (
        SP == 8 and TP == 4 and D % (SP * 128) == 0 and T % (TP * 32) == 0 and T % BLOCK == 0
        and args[1].shape[1] == TP * 128 and args[6].shape[1] == TP * 128
    )


def solution(mesh):
    in_specs = (
        P(("sp", "tp"), None),
        P("sp", "tp"),
        P("sp", "tp"),
        P("sp", "tp"),
        P("sp", "tp"),
        P("tp", "sp"),
        P("sp", "tp"),
        P("sp", "tp"),
        P("sp", "tp"),
        P("sp", "tp"),
        P("tp", "sp"),
        P("tp", None),
        P("tp", None),
        P(),
        P("sp", "tp"),
        P("tp", "sp"),
    )
    out_specs = P(("sp", "tp"), None)
    SP, TP = mesh.shape["sp"], mesh.shape["tp"]

    def layer(*args):
        body = functools.partial(one_kernel, SP, TP) if fits_kernel(SP, TP, args) else on_device
        return jax.shard_map(
            body, mesh=mesh, in_specs=in_specs, out_specs=out_specs, check_vma=False
        )(*args)

    return layer
```

profile of v0, /device:TPU:13, one launch (start us, length us, event | category | flops | bytes accessed | tf_op | source)
XLA Modules:
  0.0 206.6 jit_solution(6783226986436012211)
XLA Ops:
  0.0 0.0 copy-start
  0.0 0.0 copy-start.1
  0.0 1.3 reshape.7.gain
  1.3 0.0 copy-done
  1.3 0.0 copy-done.1
  1.4 0.6 pad.4.decay
  2.0 202.5 %shard_map.172 = bf16[192,2048]{1,0:T(8,128)(2,1)} custom-call(bf16[192,2048]{1,0:T(8,128)(2,1)} %stream.1, bf16[768,128]{1,0:T(8,128)(2,1)} %qw.1, bf16[768,128]{1,0:T(8,128)(2,1)} %kw.1, bf16[768,128]{1,0:T(8,128)(2,1)} %vw.1, bf16[768,128]{1,0:T(8,128)(2,1)} %gw.1, bf16[768,128]{1,0:T(8,128)(2,1)} %qn.1, bf16[768,128]{1,0:T(8,128)(2,1)} %kn.1, ...), custom_call_target="tpu_custom_call" | custom-call | tf_op jit(solution)/shard_map/pallas_call | solution.py:629
  204.5 2.1 %copy.20 = bf16[192,2048]{1,0:T(8,128)(2,1)} copy(bf16[192,2048]{1,0:T(8,128)(2,1)} %shard_map.172) | data formatting | bytes 1572864
  (2 shorter events, 0.0 us)
Async XLA Ops:
  0.0 1.3 copy-start
  0.0 1.3 copy-start.1
where the time goes:
time: 207 us
  Pallas kernels  203 us (98%)
  local copies, waits for them, and re-layouts  4.06 us (2%)
    pallas_call x1, Pallas kernels, one_kernel(): pl.pallas_call(functools.partial(layer_kernel, SP, TP), out_shape=jax.Sha...  203 us

commit v1 on v0

--- a/solution.py
+++ b/solution.py
@@ -232,120 +232,64 @@
     SP, TP,
     stream, qw, kw, vw, gw, qn, kn, vn, gn, decay, offs, starts, gain, ow_w, ow_n, up, down,
     out,
-    up_buf, down_buf, ow_buf, st_in, k_rot, before, inside, mixed, mix_in, mid, rows, hidden, part, part_in,
-    ssem, rsem, lsem, zsend, zrecv,
+    up_buf, down_buf, ow_buf, st_buf, k_rot, before, inside, mixed, mix_in, mid, rows, hidden, part,
+    mate_in, x_in, y_in, last_in, z_in,
+    ssem, rsem, lsem, zsend, zrecv, srecv,
 ):
     sp = lax.axis_index("sp")
     tp = lax.axis_index("tp")
     NZ = SP // 2
-    z = sp // 2
-    y = sp % 2
+    z, y = sp // 2, sp % 2
+    x, c = tp // 2, tp % 2
     T = qw.shape[0]
     NB = T // BLOCK
     RT = T // TP
+    RH = RT // 2
     RB = up.shape[0]
     CB = down.shape[1]
     D = stream.shape[1]
     FH = up.shape[1] // 2
-    mate = tp + 1 - 2 * (tp % 2)
-
-    def at(dz, dy):
-        return ((z + dz) % NZ) * 2 + (y + dy) % 2
-
+    heavy = (z == 1) | (z == 2)
+    is_end = jnp.logical_not(heavy)
+    pz = z + 1 - 2 * (z % 2)
+    mz = NZ - 1 - z
+    goal_z = jnp.where(heavy, mz, pz)
+
+    def dev(zz, dy=0, dx=0, dc=0):
+        return (zz * 2 + (y + dy) % 2, (x + dx) % 2 * 2 + (c + dc) % 2)
+
+    x_dev, y_dev, mate_dev = dev(z, 0, 1), dev(z, 1), dev(z, 0, 0, 1)
     count = [0]
     pending = []
 
-    def send(src, dst, device):
-        k = count[0]
+    def link():
         count[0] += 1
-        copy = pltpu.make_async_remote_copy(
+        return count[0] - 1
+
+    def copy_of(k, src, dst, device):
+        return pltpu.make_async_remote_copy(
             src_ref=src, dst_ref=dst, send_sem=ssem.at[k], recv_sem=rsem.at[k],
             device_id=device, device_id_type=MESH_ID,
         )
+
+    def start(k, src, dst, device):
+        copy = copy_of(k, src, dst, device)
         copy.start()
         pending.append(copy)
         return copy
 
-    def group(dy, dt):
-        return (z * 2 + (y + dy) % 2, (tp + dt) % TP)
-
-    def to_sp(i):
-        return (i, tp)
-
-    def to_tp(i):
-        return (sp, i)
+    def send(src, dst, device):
+        return start(link(), src, dst, device)
+
+    def arrive(k, dst):
+        copy_of(k, dst, dst, mate_dev).wait_recv()
 
     barrier = pltpu.get_barrier_semaphore()
-    for d in range(1, SP):
-        pl.semaphore_signal(barrier, inc=1, device_id=to_sp((sp + d) % SP), device_id_type=MESH_ID)
-    for d in range(1, TP):
-        pl.semaphore_signal(barrier, inc=1, device_id=to_tp((tp + d) % TP), device_id_type=MESH_ID)
-    for d in range(1, TP):
-        pl.semaphore_signal(barrier, inc=1, device_id=group(1, d), device_id_type=MESH_ID)
-    pl.semaphore_wait(barrier, SP + 2 * TP - 3)
-
-    def up_at(i):
-        return up_buf.at[pl.ds(pl.multiple_of(i * RB, RB), RB), :]
-
-    def down_at(i):
-        return down_buf.at[i]
-
-    place = (up_at, down_at)
-
-    def hidden_half(w, half):
-        cut = pl.ds(pl.multiple_of(half * FH, FH), FH)
-        return up.at[:, cut] if w == 0 else down.at[cut, :]
-
-    across_y = to_sp(at(0, 1))
-    line_waits = []
-
-    def piece(w, dy, zs):
-        return place[w](zs * 2 + (y + dy) % 2)
-
-    def line_copy(w, dy, zs, src, slot, device_z):
-        return pltpu.make_async_remote_copy(
-            src_ref=src, dst_ref=piece(w, dy, zs), send_sem=zsend.at[slot],
-            recv_sem=zrecv.at[(w * 2 + dy) * NZ + zs],
-            device_id=to_sp(device_z * 2 + y), device_id_type=MESH_ID,
-        )
-
-    def line_start(when, copy):
-        @pl.when(when)
-        def _():
-            copy.start()
-
-        line_waits.append((when, copy))
-
-    def line_send(w, dy):
-        for t in (1, 2, 0, 3):
-            src = hidden_half(w, y) if dy == 0 else piece(w, dy, z)
-            far = ((z == 0) & (t == 3)) | ((z == NZ - 1) & (t == 0))
-            line_start((z != t) & jnp.logical_not(far), line_copy(w, dy, z, src, (w * 2 + dy) * 5 + t, t))
-
-    def line_wait(w, dy, zs):
-        line_copy(w, dy, zs, piece(w, dy, zs), 0, (z + 1) % NZ).wait_recv()
-
-    def line_relay(w, dy):
-        for me, source, target in ((2, 0, 3), (1, 3, 0)):
-            @pl.when(z == me)
-            def _():
-                line_wait(w, dy, source)
-
-            slot = (w * 2 + dy) * 5 + 4
-            line_start(z == me, line_copy(w, dy, source, piece(w, dy, source), slot, target))
-
-    def line_arrived(w, dy, d):
-        zs = (z + d * (1 + 2 * (z // 2))) % NZ
-        relayed = ((z == 2) & (zs == 0)) | ((z == 1) & (zs == 3))
-
-        @pl.when(jnp.logical_not(relayed))
-        def _():
-            line_wait(w, dy, zs)
-
-        return zs * 2 + (y + dy) % 2
-
-    up_y = send(hidden_half(0, (y + 1) % 2), up_at(sp), across_y)
-    line_send(0, 0)
+    for d in range(1, NZ):
+        pl.semaphore_signal(barrier, inc=1, device_id=dev((z + d) % NZ), device_id_type=MESH_ID)
+    for device in (x_dev, y_dev, mate_dev, dev(z, 0, 1, 1)):
+        pl.semaphore_signal(barrier, inc=1, device_id=device, device_id_type=MESH_ID)
+    pl.semaphore_wait(barrier, NZ + 3)
 
     locals_ = []
 
@@ -353,25 +297,96 @@
         copy = pltpu.make_async_copy(src, dst, lsem.at[len(locals_)])
         copy.start()
         locals_.append(copy)
-
-    def ow_at(i, g):
-        return ow_buf.at[i, pl.ds(g * 128, 128), :]
-
-    ow_mate = [send(r, ow_at(tp, g), to_tp(mate)) for g, r in enumerate((ow_w, ow_n))]
-    ow_far = [
-        (q, g, send(r, ow_at(tp, g), to_tp((tp + 2 * q) % TP)))
-        for q in range(1, TP // 2) for g, r in enumerate((ow_w, ow_n))
+        return copy
+
+    HB = RB // 2
+    HF = FH // 2
+
+    def up_at(zs, yy, part_of):
+        return up_buf.at[pl.ds(pl.multiple_of((zs * 2 + yy) * RB + part_of * HB, HB), HB), :]
+
+    def down_at(zs, yy):
+        return down_buf.at[zs * 2 + yy]
+
+    def up_half(half, part_of):
+        return up.at[pl.ds(part_of * HB, HB), pl.ds(pl.multiple_of(half * FH, FH), FH)]
+
+    def down_half(half, part_of):
+        return down.at[pl.ds(pl.multiple_of(half * FH + part_of * HF, HF), HF), :]
+
+    z_copies = []
+
+    def z_copy(slot, sem, src, dst, zz):
+        return pltpu.make_async_remote_copy(
+            src_ref=src, dst_ref=dst, send_sem=zsend.at[slot], recv_sem=zrecv.at[sem],
+            device_id=dev(zz), device_id_type=MESH_ID,
+        )
+
+    def up_sem(zs, yy, part_of):
+        return (zs * 2 + yy) * 2 + part_of
+
+    def down_sem(zs, yy):
+        return 4 * NZ + zs * 2 + yy
+
+    z_slots = [0]
+
+    def z_slot():
+        z_slots[0] += 1
+        return z_slots[0] - 1
+
+    def up_send(zs, yy, part_of, src, zz, into):
+        copy = z_copy(z_slot(), up_sem(zs, yy, part_of), src, up_at(zs, yy, part_of), zz)
+        copy.start()
+        into.append(copy)
+
+    def down_send(zs, yy, src, zz, into):
+        copy = z_copy(z_slot(), down_sem(zs, yy), src, down_at(zs, yy), zz)
+        copy.start()
+        into.append(copy)
+
+    def up_wait(zs, yy, part_of):
+        ref = up_at(zs, yy, part_of)
+        z_copy(0, up_sem(zs, yy, part_of), ref, ref, goal_z).wait_recv()
+
+    def down_wait(zs, yy):
+        ref = down_at(zs, yy)
+        z_copy(0, down_sem(zs, yy), ref, ref, goal_z).wait_recv()
+
+    oy = 1 - y
+    ox = 1 - x
+    SW = D // 4
+
+    def ow_at(i, g, cols):
+        return ow_buf.at[i, pl.ds(g * 128, 128), cols]
+
+    def relay_cols(yy):
+        return pl.ds(pl.multiple_of(yy * 3 * SW, SW), SW)
+
+    main_cols = pl.ds(SW, 2 * SW)
+    every = pl.ds(0, D)
+    side = ox * 2 + c
+    ow_first = [
+        send(r.at[:, relay_cols(y)], ow_at(tp, g, relay_cols(y)), x_dev) for g, r in enumerate((ow_w, ow_n))
     ]
-    keep(hidden_half(0, y), up_at(sp))
-    keep(hidden_half(1, y), down_at(sp))
-    keep(ow_w, ow_at(tp, 0))
-    keep(ow_n, ow_at(tp, 1))
+    ow_main = [
+        send(r.at[:, main_cols], ow_at(tp, g, main_cols), x_dev) for g, r in enumerate((ow_w, ow_n))
+    ]
+    ow_mate = [send(r, ow_at(tp, g, every), mate_dev) for g, r in enumerate((ow_w, ow_n))]
+    up_send(z, y, 0, up_half(y, 0), goal_z, z_copies)
+    keep(ow_w, ow_at(tp, 0, every))
+    keep(ow_n, ow_at(tp, 1, every))
+    keep(up_half(y, 0), up_at(z, y, 0))
+    keep(up_half(y, 1), up_at(z, y, 1))
+    down_kept = [
+        keep(down_half(y, i), down_buf.at[sp, pl.ds(i * HF, HF), :]) for i in range(2)
+    ]
 
     lane = lax.broadcasted_iota(jnp.int32, (128, 128), 1)
     row = lax.broadcasted_iota(jnp.int32, (128, 128), 0)
     lower = row >= lane
     low = lane < HDN
     low_row = row < HDN
+    low_half = lax.broadcasted_iota(jnp.int32, (HDN, 128), 1) < HDN
     diagonal = low == low_row
     cr = decay[...]
     step = 1
@@ -402,12 +417,12 @@
         co, so = offs[2 * g], offs[2 * g + 1]
         return co * cb - so * sb, (so * cb + co * sb) * (sign_n if g else sign_w)
 
-    def turned(x, table, g):
+    def turned(v, table, g):
         if g:
-            other = jnp.where(early, pltpu.roll(x, 128 - HDN // 2, 1), pltpu.roll(x, HDN // 2, 1))
+            other = jnp.where(early, pltpu.roll(v, 128 - HDN // 2, 1), pltpu.roll(v, HDN // 2, 1))
         else:
-            other = pltpu.roll(x, HDW // 2, 1)
-        return x * table[0] + other * table[1]
+            other = pltpu.roll(v, HDW // 2, 1)
+        return v * table[0] + other * table[1]
 
     state_w = jnp.zeros((128, 128), F32)
     state_n = jnp.zeros((128, 128), F32)
@@ -429,10 +444,11 @@
         state_n = jnp.where(low_row, jnp.exp(t1), jnp.exp(t2)) * state_n + jnp.where(diagonal, grown, 0.0)
     small = lax.broadcasted_iota(jnp.int32, (16, 128), 0)
     rates = jnp.where(small == 0, jnp.exp(sums[0]), jnp.where(small == 1, jnp.exp(sums[1]), jnp.exp(sums[2])))
-    st_in[sp, 0:128, :] = state_w.astype(BF16)
-    st_in[sp, 128:256, :] = state_n.astype(BF16)
-    st_in[sp, 256:272, :] = rates.astype(BF16)
-    states = [send(st_in.at[sp], st_in.at[sp], to_sp((sp + d) % SP)) for d in range(1, SP)]
+    st_buf[0, 0:128, :] = state_w.astype(BF16)
+    st_buf[0, 128:192, :] = (state_n[0:HDN, :] + state_n[HDN:128, :]).astype(BF16)
+    st_buf[0, 192:208, :] = rates.astype(BF16)
+    state_y = send(st_buf.at[0], st_buf.at[1], y_dev)
+    cross_up = [send(up_half(oy, 0), up_at(z, y, 0), y_dev)]
 
     for b in range(NB):
         rs = pl.ds(b * BLOCK, BLOCK)
@@ -451,21 +467,59 @@
         k_rot[rs, 0:128] = (qwr * jnp.exp(col(0, b))).astype(BF16)
         k_rot[rs, 128:256] = (qnr * pair(jnp.exp(col(1, b)), jnp.exp(col(2, b)))).astype(BF16)
 
-    up_y.wait_recv()
-    line_send(0, 1)
-    down_y = send(hidden_half(1, (y + 1) % 2), down_at(sp), across_y)
-    line_send(1, 0)
-
-    for copy in states:
+    def state(i):
+        return st_buf[i, 0:128, :].astype(F32), st_buf[i, 128:192, :].astype(F32), st_buf[i, 192:208, :].astype(F32)
+
+    def chained(first, second):
+        r = second[2]
+        return (
+            first[0] * r[0:1, :] + second[0],
+            first[1] * jnp.where(low_half, r[1:2, :], r[2:3, :]) + second[1],
+            first[2] * r,
+        )
+
+    state_y.wait_recv()
+    mine, theirs = state(0), state(1)
+    lead = [jnp.where(y == 0, a, b) for a, b in zip(mine, theirs)]
+    rear = [jnp.where(y == 0, b, a) for a, b in zip(mine, theirs)]
+    plane = chained(lead, rear)
+    st_buf[2, 0:128, :] = plane[0].astype(BF16)
+    st_buf[2, 128:192, :] = plane[1].astype(BF16)
+    st_buf[2, 192:208, :] = plane[2].astype(BF16)
+
+    def state_copy(k, zs, zz):
+        return pltpu.make_async_remote_copy(
+            src_ref=st_buf.at[2], dst_ref=st_buf.at[3 + zs], send_sem=ssem.at[k], recv_sem=srecv.at[zs],
+            device_id=dev(zz), device_id_type=MESH_ID,
+        )
+
+    state_sends = []
+    for d in range(NZ - 1, 0, -1):
+        copy = state_copy(link(), z, (z + d) % NZ)
+        state_sends.append((z + d < NZ, copy))
+
+        @pl.when(z + d < NZ)
+        def _(copy=copy):
+            copy.start()
+
+    up_send(z, y, 1, up_half(y, 1), goal_z, z_copies)
+    for copy in ow_first:
         copy.wait_recv()
-    s_w = jnp.zeros((128, 128), F32)
-    s_n = jnp.zeros((128, 128), F32)
-    for j in range(SP):
-        r = st_in[j, 256:272, :].astype(F32)
-        s_w = jnp.where(j < sp, s_w * r[0:1, :] + st_in[j, 0:128, :].astype(F32), s_w)
-        s_n = jnp.where(
-            j < sp, s_n * jnp.where(low_row, r[1:2, :], r[2:3, :]) + st_in[j, 128:256, :].astype(F32), s_n
-        )
+    ow_y = send(ow_buf.at[side, :, relay_cols(y)], ow_buf.at[side, :, relay_cols(y)], y_dev)
+    cross_up.append(send(up_half(oy, 1), up_at(z, y, 1), y_dev))
+    ow_hand = [send(ow_buf.at[side, :, relay_cols(y)], ow_buf.at[side, :, relay_cols(y)], mate_dev)]
+
+    for zs in range(NZ - 1):
+        @pl.when(zs < z)
+        def _(zs=zs):
+            state_copy(0, zs, mz).wait_recv()
+
+    held = (jnp.zeros((128, 128), F32), jnp.zeros((HDN, 128), F32), jnp.zeros((16, 128), F32))
+    for zs in range(NZ - 1):
+        held = [jnp.where(zs < z, a, b) for a, b in zip(chained(held, state(3 + zs)), held)]
+    held = [jnp.where(y == 1, a, b) for a, b in zip(chained(held, theirs), held)]
+    s_w = held[0]
+    s_n = jnp.concatenate([jnp.where(low_half, held[1], 0.0), jnp.where(low_half, 0.0, held[1])], axis=0)
 
     sums = [jnp.zeros((1, 1), F32) for _ in range(3)]
     for b in range(NB):
@@ -476,9 +530,9 @@
         o_w = inside[rs, 0:128] + dot(k_rot[rs, 0:128], whole_w.astype(BF16))
         o_n = inside[rs, 128:256] + dot(k_rot[rs, 128:256], whole_n.astype(BF16))
 
-        def both(x):
-            first = jnp.sum(jnp.where(low, x, 0.0), axis=-1, keepdims=True) / HDN
-            second = jnp.sum(jnp.where(low, 0.0, x), axis=-1, keepdims=True) / HDN
+        def both(v):
+            first = jnp.sum(jnp.where(low, v, 0.0), axis=-1, keepdims=True) / HDN
+            second = jnp.sum(jnp.where(low, 0.0, v), axis=-1, keepdims=True) / HDN
             return pair(first, second)
 
         c_w = o_w - jnp.mean(o_w, axis=-1, keepdims=True)
@@ -492,123 +546,357 @@
         return pl.ds(pl.multiple_of(i * RT, RT), RT)
 
     swaps = [
-        send(mixed.at[my_rows((tp + d) % TP), :], mix_in.at[tp], to_tp((tp + d) % TP)) for d in range(1, TP)
+        send(mixed.at[my_rows((x + dx) % 2 * 2 + (c + dc) % 2), :], mix_in.at[tp], dev(z, 0, dx, dc))
+        for dx, dc in ((1, 0), (1, 1), (0, 1))
+    ]
+    cross_down = [
+        send(down_half(oy, 0), down_buf.at[sp, pl.ds(0, HF), :], y_dev)
     ]
     mix_in[tp] = mixed[my_rows(tp), :]
-    ow_relay = []
-    for q, g, copy in ow_far:
+    cross_up[0].wait_recv()
+    up_send(z, oy, 0, up_at(z, oy, 0), goal_z, z_copies)
+    for copy in ow_main:
         copy.wait_recv()
-        came = (tp + TP - 2 * q) % TP
-        ow_relay.append(send(ow_at(came, g), ow_at(came, g), to_tp(mate)))
-    line_relay(0, 0)
-    for copy in swaps + ow_mate + ow_relay:
+    ow_hand.append(send(ow_buf.at[side, :, main_cols], ow_buf.at[side, :, main_cols], mate_dev))
+    ow_y.wait_recv()
+    ow_hand.append(send(ow_buf.at[side, :, relay_cols(oy)], ow_buf.at[side, :, relay_cols(oy)], mate_dev))
+    for copy in ow_mate + ow_hand + swaps:
         copy.wait_recv()
     for copy in locals_:
         copy.wait()
 
-    def project(c, _):
-        cs = pl.ds(pl.multiple_of(c * 512, 512), 512)
+    def project(i, _):
+        cs = pl.ds(pl.multiple_of(i * 512, 512), 512)
         acc = stream[:, cs].astype(F32)
-        for i in range(TP):
-            acc = acc + dot(mix_in[i], ow_buf[i, :, cs])
+        for j in range(TP):
+            acc = acc + dot(mix_in[j], ow_buf[j, :, cs])
         mid[:, cs] = acc.astype(BF16)
         return 0
 
     lax.fori_loop(0, D // 512, project, 0)
 
+    own_set = jnp.where(heavy, 0, 1)
+
+    def unit(s, dy, dx, h, dc=0):
+        return (((s * 2 + (y + dy) % 2) * 2 + (x + dx) % 2) * 2 + h) * 2 + (c + dc) % 2
+
+    NS = 32
+
     def norm(i, _):
-        m = mid[pl.ds(pl.multiple_of(i * 32, 32), 32), :].astype(F32)
+        m = mid[pl.ds(pl.multiple_of(i * NS, NS), NS), :].astype(F32)
         scale = lax.rsqrt(jnp.mean(m * m, axis=-1, keepdims=True) + norm_eps)
-        rows[pl.ds(pl.multiple_of((y * TP + tp) * RT + i * 32, 32), 32), :] = (m * scale * gain[...].astype(F32)).astype(BF16)
+        per = RH // NS
+        rows[unit(own_set, 0, 0, i // per), pl.ds(pl.multiple_of(i % per * NS, NS), NS), :] = (
+            m * scale * gain[...].astype(F32)
+        ).astype(BF16)
         return 0
 
-    lax.fori_loop(0, RT // 32, norm, 0)
-
-    def block(dy, dt):
-        return rows.at[my_rows((y + dy) % 2 * TP + (tp + dt) % TP), :]
-
-    near_x = send(block(0, 0), block(0, 0), group(0, 2))
-    near_y = send(block(0, 0), block(0, 0), group(1, 0))
-    hand = [send(block(0, 0), block(0, 0), to_tp(mate))]
-    line_relay(0, 1)
-    down_y.wait_recv()
-    line_send(1, 1)
-    near_x.wait_recv()
-    corner = send(block(0, 2), block(0, 2), group(1, 0))
-    hand.append(send(block(0, 2), block(0, 2), to_tp(mate)))
-    near_y.wait_recv()
-    hand.append(send(block(1, 0), block(1, 0), to_tp(mate)))
-    for dy in range(2):
-        for d in range(1, NZ):
-            line_arrived(0, dy, d)
-
-    def up_rows(dy, dp):
-        i = (y + dy) % 2 * (TP // 2) + (tp // 2 + dp) % (TP // 2)
-        rs = pl.ds(pl.multiple_of(i * 2 * RT, 2 * RT), 2 * RT)
-
-        def one(c, _):
-            cs = pl.ds(pl.multiple_of(c * 512, 512), 512)
-            h = jnp.maximum(dot(rows[rs, :], up_buf[:, cs]), 0.0)
-            hidden[rs, cs] = (h * h).astype(BF16)
-            return 0
-
-        lax.fori_loop(0, FH // 512, one, 0)
-
-    hand[0].wait_recv()
-    up_rows(0, 0)
-    corner.wait_recv()
-    hand.append(send(block(1, 2), block(1, 2), to_tp(mate)))
-    line_relay(1, 0)
-    hand[1].wait_recv()
-    up_rows(0, 1)
-    hand[2].wait_recv()
-    up_rows(1, 0)
-    hand[3].wait_recv()
-    up_rows(1, 1)
-
-    peers = [(dy, dt) for dy in range(2) for dt in range(TP) if dy or dt]
-
-    def chunk(k, j):
-        def one(i, _):
-            rs = pl.ds(pl.multiple_of(i * 2 * RT, 2 * RT), 2 * RT)
-            part[k, rs, :] = dot(hidden[rs, :], down_buf[j]).astype(BF16)
-            return 0
-
-        lax.fori_loop(0, TP, one, 0)
-        return [
-            send(
-                part.at[k, my_rows((y + dy) % 2 * TP + (tp + dt) % TP), :],
-                part_in.at[k, dy * TP + dt - 1], group(dy, dt),
-            )
-            for dy, dt in peers
-        ]
-
-    def finish(k, j, copies):
-        for copy in copies:
+    lax.fori_loop(0, RT // NS, norm, 0)
+
+    def piece(s, dy, dx, h):
+        return rows.at[unit(s, dy, dx, h)]
+
+    def pass_on(s, dy, dx, h, device):
+        return send(piece(s, dy, dx, h), piece(s, dy, dx, h), device)
+
+    z_units = [(link(), u) for u in ((0, 0, 0), (0, 0, 1), (0, 1, 0), (1, 0, 1))]
+    z_parts = [(link(), link()) for _ in range(SP)]
+    common = list(pending)
+    pending.clear()
+
+    def cols_of(j):
+        return pl.ds(pl.multiple_of(j * CB, CB), CB)
+
+    def put(j, h, a, b):
+        rs = pl.ds(h * RH, RH)
+        out[rs, cols_of(j)] = (mid[rs, cols_of(j)].astype(F32) + a.astype(F32) + b.astype(F32)).astype(BF16)
+
+    @pl.when(is_end)
+    def _():
+        sent = []
+
+        def z_unit(i):
+            k, (dy, dx, h) = z_units[i]
+            start(k, piece(1, dy, dx, h), piece(1, dy, dx, h), dev(pz))
+
+        side_x = pass_on(1, 0, 0, 0, x_dev)
+        side_y = pass_on(1, 0, 0, 1, y_dev)
+        cross_up[1].wait_recv()
+        up_send(z, oy, 1, up_at(z, oy, 1), goal_z, sent)
+        z_unit(0)
+        z_unit(1)
+        cross_down.append(
+            send(down_half(oy, 1), down_buf.at[sp, pl.ds(HF, HF), :], y_dev)
+        )
+        side_x.wait_recv()
+        z_unit(2)
+        side_y.wait_recv()
+        z_unit(3)
+        for copy in cross_down:
             copy.wait_recv()
-        cs = pl.ds(pl.multiple_of(j * CB, CB), CB)
-        acc = mid[:, cs].astype(F32) + part[k, my_rows(y * TP + tp), :].astype(F32)
-        for d in range(2 * TP - 1):
-            acc = acc + part_in[k, d].astype(F32)
-        out[:, cs] = acc.astype(BF16)
-
-    done = []
-    for k in range(SP):
-        d, dy = k // 2, (y + k) % 2
-        if k == 4:
-            line_relay(1, 1)
-        j = line_arrived(1, dy, d) if d else at(0, dy)
-        done.append((k, j, chunk(k, j)))
-        if k > 1:
-            finish(*done[k - 2])
-    finish(*done[-2])
-    finish(*done[-1])
-    for when, copy in line_waits:
+        for yy in range(2):
+            down_send(z, yy, down_at(z, yy), goal_z, sent)
+        order = [(zs, yy) for zs in (pz, NZ - 1 - pz, z, NZ - 1 - z) for yy in range(2)]
+        done = []
+        for k, (zs, yy) in enumerate(order):
+            ka, kb = z_parts[k]
+            arrive(ka, z_in.at[k, 0])
+            a = send(z_in.at[k, 0, oy], last_in.at[k, 0], y_dev)
+            arrive(kb, z_in.at[k, 1])
+            b = send(z_in.at[k, 1, ox], last_in.at[k, 1], x_dev)
+            done.append((k, zs * 2 + yy, a, b))
+            if k:
+                end_finish(done[k - 1], z_in, last_in, put, x, y)
+        end_finish(done[-1], z_in, last_in, put, x, y)
+        for copy in sent + pending:
+            copy.wait_send()
+        pending.clear()
+        cross_down.pop()
+
+    @pl.when(heavy)
+    def _():
+        sent = []
+        hands = {}
+
+        def hand(s, dy, dx, h):
+            hands[s, dy, dx, h] = pass_on(s, dy, dx, h, mate_dev)
+
+        def z_arrive(i):
+            k, (dy, dx, h) = z_units[i]
+            arrive(k, piece(1, dy, dx, h))
+            return pass_on(1, dy, dx, h, x_dev if h else y_dev)
+
+        def up_relay(yy):
+            for i in range(2):
+                up_wait(pz, yy, i)
+                up_send(pz, yy, i, up_at(pz, yy, i), mz, sent)
+
+        xa = pass_on(0, 0, 0, 0, x_dev)
+        yb = pass_on(0, 0, 0, 1, y_dev)
+        xb = pass_on(0, 0, 0, 1, x_dev)
+        ya = pass_on(0, 0, 0, 0, y_dev)
+        hand(0, 0, 0, 0)
+        hand(0, 0, 0, 1)
+        cross_down.append(
+            send(down_half(oy, 1), down_buf.at[sp, pl.ds(HF, HF), :], y_dev)
+        )
+        up_relay(y)
+        cross_up[1].wait_recv()
+        up_send(z, oy, 1, up_at(z, oy, 1), goal_z, sent)
+        xa.wait_recv()
+        corner_a = pass_on(0, 0, 1, 0, y_dev)
+        hand(0, 0, 1, 0)
+        yb.wait_recv()
+        corner_b = pass_on(0, 1, 0, 1, x_dev)
+        hand(0, 1, 0, 1)
+        up_relay(oy)
+        down_send(z, y, down_at(z, y), goal_z, sent)
+        ends = {}
+        ends[1, 0, 0] = z_arrive(0)
+        hand(1, 0, 0, 0)
+        xb.wait_recv()
+        hand(0, 0, 1, 1)
+        ya.wait_recv()
+        hand(0, 1, 0, 0)
+        ends[0, 1, 1] = z_arrive(1)
+        hand(1, 0, 0, 1)
+        for copy in cross_down:
+            copy.wait_recv()
+        down_send(z, oy, down_at(z, oy), goal_z, sent)
+        corner_a.wait_recv()
+        hand(0, 1, 1, 0)
+        corner_b.wait_recv()
+        hand(0, 1, 1, 1)
+        for zs in (mz, NZ - 1 - pz):
+            for yy in range(2):
+                for i in range(2):
+                    up_wait(zs, yy, i)
+
+        def up_rows(s, dy, dx):
+            for h in range(2):
+                hands[s, dy, dx, h].wait_recv()
+            i = (s * 2 + (y + dy) % 2) * 2 + (x + dx) % 2
+            us = pl.ds(pl.multiple_of(i * 4, 4), 4)
+
+            def one(j, _):
+                cs = pl.ds(pl.multiple_of(j * 512, 512), 512)
+                h = jnp.maximum(dot(rows[us].reshape(2 * RT, D), up_buf[:, cs]), 0.0)
+                hidden[i, :, cs] = (h * h).astype(BF16)
+                return 0
+
+            lax.fori_loop(0, FH // 512, one, 0)
+
+        up_rows(0, 0, 0)
+        ends[1, 1, 0] = z_arrive(2)
+        hand(1, 0, 1, 0)
+        up_rows(0, 0, 1)
+        ends[1, 1, 1] = z_arrive(3)
+        hand(1, 1, 0, 1)
+        up_rows(0, 1, 0)
+        up_rows(0, 1, 1)
+
+        chain = (z, mz, pz, NZ - 1 - pz)
+        chunks = (
+            [(0, 0, yy) for yy in range(2)] + [(0, 1, yy) for yy in range(2)]
+            + [(1, 0, yy) for yy in range(2)] + [(1, 1, yy) for yy in range(2)]
+            + [(s, i, yy) for i in (2, 3) for yy in range(2) for s in range(2)]
+        )
+        waited = set()
+        relays = []
+        slots = part.shape[0]
+        stage = [dict() for _ in chunks]
+        of_set = [sum(1 for t in chunks[:k] if t[0] == chunks[k][0]) for k in range(len(chunks))]
+
+        def down_ready(i, yy):
+            if (i, yy) in waited or i == 0:
+                return
+            waited.add((i, yy))
+            down_wait(chain[i], yy)
+            if i == 2:
+                down_send(pz, yy, down_at(pz, yy), mz, sent)
+
+        def multiply(k):
+            s, i, yy = chunks[k]
+            down_ready(i, yy)
+            if k >= slots:
+                for copy in stage[k - slots]["sent"]:
+                    copy.wait_send()
+            j = chain[i] * 2 + yy
+            slot = k % slots
+
+            def one(q, _):
+                got = dot(hidden[s * 4 + q], down_buf[j]).astype(BF16)
+                part[slot, q // 2, q % 2] = got.reshape(2, 2, RH, CB)
+                return 0
+
+            lax.fori_loop(0, 4, one, 0)
+            mate = copy_of(link(), part.at[slot, :, :, :, 1 - c], mate_in.at[k], mate_dev)
+            mate.start()
+            stage[k]["mate"] = mate
+            stage[k]["sent"] = [mate]
+
+        def fold(k):
+            slot = k % slots
+            stage[k]["mate"].wait_recv()
+
+            def one(q, _):
+                for h in range(2):
+                    part[slot, q // 2, q % 2, h, c] = (
+                        part[slot, q // 2, q % 2, h, c].astype(F32) + mate_in[k, q // 2, q % 2, h].astype(F32)
+                    ).astype(BF16)
+                return 0
+
+            lax.fori_loop(0, 4, one, 0)
+            to_x = copy_of(link(), part.at[slot, :, ox, 0, c], x_in.at[k], x_dev)
+            to_x.start()
+            to_y = copy_of(link(), part.at[slot, oy, :, 1, c], y_in.at[k], y_dev)
+            to_y.start()
+            stage[k]["x"], stage[k]["y"] = to_x, to_y
+            stage[k]["sent"] += [to_x, to_y]
+
+        def spread(k):
+            slot = k % slots
+            s = chunks[k][0]
+            stage[k]["x"].wait_recv()
+            for i in range(2):
+                part[slot, i, x, 0, c] = (
+                    part[slot, i, x, 0, c].astype(F32) + x_in[k, i].astype(F32)
+                ).astype(BF16)
+            n = of_set[k]
+            if s:
+                a = copy_of(z_parts[n][0], part.at[slot, :, x, 0, c], z_in.at[n, 0], dev(pz))
+            else:
+                a = copy_of(link(), part.at[slot, oy, x, 0, c], last_in.at[n, 0], y_dev)
+            a.start()
+            stage[k]["y"].wait_recv()
+            for i in range(2):
+                part[slot, y, i, 1, c] = (
+                    part[slot, y, i, 1, c].astype(F32) + y_in[k, i].astype(F32)
+                ).astype(BF16)
+            if s:
+                b = copy_of(z_parts[n][1], part.at[slot, y, :, 1, c], z_in.at[n, 1], dev(pz))
+            else:
+                b = copy_of(link(), part.at[slot, y, ox, 1, c], last_in.at[n, 1], x_dev)
+            b.start()
+            stage[k]["last"] = (a, b)
+            stage[k]["sent"] += [a, b]
+
+        def finish(k):
+            s, i, yy = chunks[k]
+            if s:
+                return
+            slot = k % slots
+            n = of_set[k]
+            j = chain[i] * 2 + yy
+            for h, copy in enumerate(stage[k]["last"]):
+                copy.wait_recv()
+                put(j, h, part[slot, y, x, h, c], last_in[n, h])
+
+        reached = [0, 0, 0]
+
+        def advance(which, limit):
+            for k in range(reached[which], max(limit, reached[which])):
+                (fold, spread, finish)[which](k)
+            reached[which] = max(limit, reached[which])
+
+        n_chunks = len(chunks)
+        for k in range(n_chunks):
+            if k == 4:
+                advance(0, k)
+                ends[1, 0, 0].wait_recv()
+                hand(1, 1, 0, 0)
+                ends[0, 1, 1].wait_recv()
+                hand(1, 0, 1, 1)
+                up_rows(1, 0, 0)
+                advance(1, 1)
+                up_rows(1, 0, 1)
+                advance(1, 2)
+                ends[1, 1, 0].wait_recv()
+                hand(1, 1, 1, 0)
+                ends[1, 1, 1].wait_recv()
+                hand(1, 1, 1, 1)
+                up_rows(1, 1, 0)
+                advance(1, 3)
+                up_rows(1, 1, 1)
+                down_ready(2, 0)
+            elif k in (10, 12, 14):
+                advance(0, k)
+                advance(1, k - 1)
+                advance(2, k - 3)
+            else:
+                advance(2, k - 6)
+                advance(1, k - 4)
+                advance(0, k - 2)
+            if k == 7:
+                down_ready(2, 1)
+            multiply(k)
+        for k in range(n_chunks - 2, n_chunks + 1):
+            advance(0, k)
+            advance(1, k - 1)
+            advance(2, k - 3)
+        advance(1, n_chunks)
+        advance(2, n_chunks)
+        for k in range(n_chunks - slots, n_chunks):
+            for copy in stage[k]["sent"]:
+                copy.wait_send()
+        for copy in sent + pending:
+            copy.wait_send()
+        pending.clear()
+
+    for when, copy in state_sends:
         @pl.when(when)
         def _(copy=copy):
             copy.wait_send()
-    for copy in pending:
+    for copy in common + z_copies:
         copy.wait_send()
+
+
+def end_finish(one, z_in, last_in, put, x, y):
+    k, j, a, b = one
+    a.wait_recv()
+    put(j, 0, z_in[k, 0, y], last_in[k, 0])
+    b.wait_recv()
+    put(j, 1, z_in[k, 1, x], last_in[k, 1])
 
 
 def one_kernel(SP, TP, *args):
@@ -617,6 +905,7 @@
     NB = T // BLOCK
     D = stream.shape[1]
     RT = T // TP
+    RH = RT // 2
     FH = up.shape[1] // 2
     CB = down.shape[1]
     heads = dw.shape[0] + dn.shape[0]
@@ -625,7 +914,7 @@
     offs, starts = turn_tables(SP, T)
     vmem = pl.BlockSpec(memory_space=pltpu.VMEM)
     hbm = pl.BlockSpec(memory_space=pl.ANY)
-    copies = 96
+    copies = 256
     return pl.pallas_call(
         functools.partial(layer_kernel, SP, TP),
         out_shape=jax.ShapeDtypeStruct((RT, D), BF16),
@@ -635,25 +924,30 @@
             pltpu.VMEM((D, FH), BF16),
             pltpu.VMEM((SP, FH, CB), BF16),
             pltpu.VMEM((TP, 256, D), BF16),
-            pltpu.VMEM((SP, 272, 128), BF16),
+            pltpu.VMEM((7, 208, 128), BF16),
             pltpu.VMEM((T, 256), BF16),
             pltpu.VMEM((2, NB, 128, 128), F32),
             pltpu.VMEM((T, 256), F32),
             pltpu.VMEM((T, 256), BF16),
             pltpu.VMEM((TP, RT, 256), BF16),
             pltpu.VMEM((RT, D), BF16),
-            pltpu.VMEM((2 * T, D), BF16),
-            pltpu.VMEM((2 * T, FH), BF16),
-            pltpu.VMEM((SP, 2 * T, CB), BF16),
-            pltpu.VMEM((SP, 2 * TP - 1, RT, CB), BF16),
+            pltpu.VMEM((32, RH, D), BF16),
+            pltpu.VMEM((8, 2 * RT, FH), BF16),
+            pltpu.VMEM((8, 2, 2, 2, 2, RH, CB), BF16),
+            pltpu.VMEM((2 * SP, 2, 2, 2, RH, CB), BF16),
+            pltpu.VMEM((2 * SP, 2, RH, CB), BF16),
+            pltpu.VMEM((2 * SP, 2, RH, CB), BF16),
+            pltpu.VMEM((SP, 2, RH, CB), BF16),
+            pltpu.VMEM((SP, 2, 2, RH, CB), BF16),
             pltpu.SemaphoreType.DMA((copies,)),
             pltpu.SemaphoreType.DMA((copies,)),
+            pltpu.SemaphoreType.DMA((8,)),
+            pltpu.SemaphoreType.DMA((24,)),
+            pltpu.SemaphoreType.DMA((24,)),
             pltpu.SemaphoreType.DMA((4,)),
-            pltpu.SemaphoreType.DMA((20,)),
-            pltpu.SemaphoreType.DMA((2 * SP,)),
         ],
         compiler_params=pltpu.CompilerParams(
-            collective_id=0, has_side_effects=True, vmem_limit_bytes=60 * 1024 * 1024
+            collective_id=0, has_side_effects=True, vmem_limit_bytes=63 * 1024 * 1024
         ),
     )(stream, qw, kw, vw, gw, qn, kn, vn, gn, decay, jnp.asarray(offs), jnp.asarray(starts),
       gain.reshape(1, D), ow, on, up, down)

time: 207 us -> 161 us (0.78)
  the two profiles are of different devices: /device:TPU:13 before, /device:TPU:0 now
where the time goes in v1:
time: 161 us; the launch traced here: 160 us
  Pallas kernels  156 us (97%)
  local copies, waits for them, and re-layouts  4.06 us (3%)
    pallas_call x1, Pallas kernels, one_kernel(): pl.pallas_call(functools.partial(layer_kernel, SP, TP), out_shape=jax.Sha...  156 us

profile of v1, /device:TPU:0, one launch (start us, length us, event | category | flops | bytes accessed | tf_op | source)
XLA Modules:
  0.0 160.3 jit_solution(4818750580278278398)
XLA Ops:
  0.0 0.0 copy-start
  0.0 0.0 copy-start.1
  0.0 1.3 reshape.7.gain
  1.3 0.0 copy-done
  1.3 0.0 copy-done.1
  1.4 0.6 pad.4.decay
  2.0 156.3 %shard_map.172 = bf16[192,2048]{1,0:T(8,128)(2,1)} custom-call(bf16[192,2048]{1,0:T(8,128)(2,1)} %stream.1, bf16[768,128]{1,0:T(8,128)(2,1)} %qw.1, bf16[768,128]{1,0:T(8,128)(2,1)} %kw.1, bf16[768,128]{1,0:T(8,128)(2,1)} %vw.1, bf16[768,128]{1,0:T(8,128)(2,1)} %gw.1, bf16[768,128]{1,0:T(8,128)(2,1)} %qn.1, bf16[768,128]{1,0:T(8,128)(2,1)} %kn.1, ...), custom_call_target="tpu_custom_call" | custom-call | tf_op jit(solution)/shard_map/pallas_call | solution.py:918
  158.3 2.1 %copy.20 = bf16[192,2048]{1,0:T(8,128)(2,1)} copy(bf16[192,2048]{1,0:T(8,128)(2,1)} %shard_map.172) | data formatting | bytes 1572864
  (2 shorter events, 0.0 us)
Async XLA Ops:
  0.0 1.3 copy-start
  0.0 1.3 copy-start.1

commit v2 on v1

--- a/solution.py
+++ b/solution.py
@@ -228,12 +228,38 @@
     return lax.dot_general(a, b, (((1,), (1,)), ((), ())), preferred_element_type=F32)
 
 
+N_CHUNKS = 16
+OWN_LEAD = 4
+SLOTS = 8
+
+
+def chunk_at(k):
+    t = k - OWN_LEAD
+    if isinstance(k, int):
+        if t < 0:
+            return 0, k // 2, k % 2
+        far = t % 3 != 2 if t < 8 else t < 10
+        n = (t - t // 3 if far else 4 + t // 3) if t < 8 else (t - 2 if far else t - 4)
+        return int(far), n // 2, n % 2
+    far = jnp.where(t < 8, jnp.where(t % 3 != 2, 1, 0), jnp.where(t < 10, 1, 0)) == 1
+    early = jnp.where(far, t - t // 3, 4 + t // 3)
+    n = jnp.where(t < 0, k, jnp.where(t < 8, early, jnp.where(far, t - 2, t - 4)))
+    return jnp.where((t >= 0) & far, 1, 0), n // 2, n % 2
+
+
+def chunk_kind(k):
+    s, i, yy = chunk_at(k)
+    n = i * 2 + yy
+    last = (s == 1) & (yy == 1) & (i < 3)
+    return s, n, last
+
+
 def layer_kernel(
     SP, TP,
-    stream, qw, kw, vw, gw, qn, kn, vn, gn, decay, offs, starts, gain, ow_w, ow_n, up, down,
+    stream, qw, kw, vw, gw, qn, kn, vn, gn, dw, dn, offs, starts, gain, ow_w, ow_n, up, down,
     out,
     up_buf, down_buf, ow_buf, st_buf, k_rot, before, inside, mixed, mix_in, mid, rows, hidden, part,
-    mate_in, x_in, y_in, last_in, z_in,
+    mate_in, x_in, y_in, last_in, z_in, z_done, rates_buf, up_sum,
     ssem, rsem, lsem, zsend, zrecv, srecv,
 ):
     sp = lax.axis_index("sp")
@@ -305,8 +331,8 @@
     def up_at(zs, yy, part_of):
         return up_buf.at[pl.ds(pl.multiple_of((zs * 2 + yy) * RB + part_of * HB, HB), HB), :]
 
-    def down_at(zs, yy):
-        return down_buf.at[zs * 2 + yy]
+    def down_at(zs, yy, part_of):
+        return down_buf.at[zs * 2 + yy, pl.ds(part_of * HF, HF), :]
 
     def up_half(half, part_of):
         return up.at[pl.ds(part_of * HB, HB), pl.ds(pl.multiple_of(half * FH, FH), FH)]
@@ -325,8 +351,8 @@
     def up_sem(zs, yy, part_of):
         return (zs * 2 + yy) * 2 + part_of
 
-    def down_sem(zs, yy):
-        return 4 * NZ + zs * 2 + yy
+    def down_sem(zs, yy, part_of):
+        return 4 * NZ + up_sem(zs, yy, part_of)
 
     z_slots = [0]
 
@@ -339,8 +365,9 @@
         copy.start()
         into.append(copy)
 
-    def down_send(zs, yy, src, zz, into):
-        copy = z_copy(z_slot(), down_sem(zs, yy), src, down_at(zs, yy), zz)
+    def down_send(zs, yy, part_of, zz, into):
+        ref = down_at(zs, yy, part_of)
+        copy = z_copy(z_slot(), down_sem(zs, yy, part_of), ref, ref, zz)
         copy.start()
         into.append(copy)
 
@@ -348,21 +375,22 @@
         ref = up_at(zs, yy, part_of)
         z_copy(0, up_sem(zs, yy, part_of), ref, ref, goal_z).wait_recv()
 
-    def down_wait(zs, yy):
-        ref = down_at(zs, yy)
-        z_copy(0, down_sem(zs, yy), ref, ref, goal_z).wait_recv()
+    def down_wait(zs, yy, part_of):
+        ref = down_at(zs, yy, part_of)
+        z_copy(0, down_sem(zs, yy, part_of), ref, ref, goal_z).wait_recv()
 
     oy = 1 - y
     ox = 1 - x
-    SW = D // 4
+    RW = D * 3 // 8
+    QB = HB // 4
 
     def ow_at(i, g, cols):
         return ow_buf.at[i, pl.ds(g * 128, 128), cols]
 
     def relay_cols(yy):
-        return pl.ds(pl.multiple_of(yy * 3 * SW, SW), SW)
-
-    main_cols = pl.ds(SW, 2 * SW)
+        return pl.ds(pl.multiple_of(yy * (D - RW), 128), RW)
+
+    main_cols = pl.ds(RW, D - 2 * RW)
     every = pl.ds(0, D)
     side = ox * 2 + c
     ow_first = [
@@ -377,9 +405,16 @@
     keep(ow_n, ow_at(tp, 1, every))
     keep(up_half(y, 0), up_at(z, y, 0))
     keep(up_half(y, 1), up_at(z, y, 1))
-    down_kept = [
-        keep(down_half(y, i), down_buf.at[sp, pl.ds(i * HF, HF), :]) for i in range(2)
-    ]
+    for i in range(2):
+        keep(down_half(y, i), down_at(z, y, i))
+
+    def cross_rows(first, many):
+        return send(
+            up.at[pl.ds(first, many), pl.ds(pl.multiple_of(oy * FH, FH), FH)],
+            up_buf.at[pl.ds(pl.multiple_of(sp * RB + first, QB), many), :], y_dev,
+        )
+
+    cross_first = [cross_rows(0, QB)]
 
     lane = lax.broadcasted_iota(jnp.int32, (128, 128), 1)
     row = lax.broadcasted_iota(jnp.int32, (128, 128), 0)
@@ -388,7 +423,12 @@
     low_row = row < HDN
     low_half = lax.broadcasted_iota(jnp.int32, (HDN, 128), 1) < HDN
     diagonal = low == low_row
-    cr = decay[...]
+    for h in range(3):
+        for b in range(NB):
+            ref = dw if h == 0 else dn
+            at = 0 if h == 0 else h - 1
+            rates_buf[h * NB + b:h * NB + b + 1, :] = ref[at:at + 1, b * BLOCK:(b + 1) * BLOCK]
+    cr = rates_buf[...]
     step = 1
     while step < 128:
         cr = cr + jnp.where(lane >= step, pltpu.roll(cr, step, 1), 0.0)
@@ -448,7 +488,7 @@
     st_buf[0, 128:192, :] = (state_n[0:HDN, :] + state_n[HDN:128, :]).astype(BF16)
     st_buf[0, 192:208, :] = rates.astype(BF16)
     state_y = send(st_buf.at[0], st_buf.at[1], y_dev)
-    cross_up = [send(up_half(oy, 0), up_at(z, y, 0), y_dev)]
+    cross_first.append(cross_rows(QB, HB - QB))
 
     for b in range(NB):
         rs = pl.ds(b * BLOCK, BLOCK)
@@ -503,12 +543,16 @@
             copy.start()
 
     up_send(z, y, 1, up_half(y, 1), goal_z, z_copies)
-    for copy in ow_first:
+    ow_y = []
+    for g, copy in enumerate(ow_first):
         copy.wait_recv()
-    ow_y = send(ow_buf.at[side, :, relay_cols(y)], ow_buf.at[side, :, relay_cols(y)], y_dev)
-    cross_up.append(send(up_half(oy, 1), up_at(z, y, 1), y_dev))
+        ow_y.append(send(ow_at(side, g, relay_cols(y)), ow_at(side, g, relay_cols(y)), y_dev))
+    cross_last = send(up_half(oy, 1), up_at(z, y, 1), y_dev)
     ow_hand = [send(ow_buf.at[side, :, relay_cols(y)], ow_buf.at[side, :, relay_cols(y)], mate_dev)]
 
+    for copy in cross_first:
+        copy.wait_recv()
+    up_send(z, oy, 0, up_at(z, oy, 0), goal_z, z_copies)
     for zs in range(NZ - 1):
         @pl.when(zs < z)
         def _(zs=zs):
@@ -549,16 +593,12 @@
         send(mixed.at[my_rows((x + dx) % 2 * 2 + (c + dc) % 2), :], mix_in.at[tp], dev(z, 0, dx, dc))
         for dx, dc in ((1, 0), (1, 1), (0, 1))
     ]
-    cross_down = [
-        send(down_half(oy, 0), down_buf.at[sp, pl.ds(0, HF), :], y_dev)
-    ]
     mix_in[tp] = mixed[my_rows(tp), :]
-    cross_up[0].wait_recv()
-    up_send(z, oy, 0, up_at(z, oy, 0), goal_z, z_copies)
     for copy in ow_main:
         copy.wait_recv()
     ow_hand.append(send(ow_buf.at[side, :, main_cols], ow_buf.at[side, :, main_cols], mate_dev))
-    ow_y.wait_recv()
+    for copy in ow_y:
+        copy.wait_recv()
     ow_hand.append(send(ow_buf.at[side, :, relay_cols(oy)], ow_buf.at[side, :, relay_cols(oy)], mate_dev))
     for copy in ow_mate + ow_hand + swaps:
         copy.wait_recv()
@@ -587,71 +627,110 @@
         scale = lax.rsqrt(jnp.mean(m * m, axis=-1, keepdims=True) + norm_eps)
         per = RH // NS
         rows[unit(own_set, 0, 0, i // per), pl.ds(pl.multiple_of(i % per * NS, NS), NS), :] = (
-            m * scale * gain[...].astype(F32)
+            m * scale * gain[...].reshape(1, D).astype(F32)
         ).astype(BF16)
         return 0
 
     lax.fori_loop(0, RT // NS, norm, 0)
 
-    def piece(s, dy, dx, h):
-        return rows.at[unit(s, dy, dx, h)]
-
-    def pass_on(s, dy, dx, h, device):
-        return send(piece(s, dy, dx, h), piece(s, dy, dx, h), device)
-
-    z_units = [(link(), u) for u in ((0, 0, 0), (0, 0, 1), (0, 1, 0), (1, 0, 1))]
-    z_parts = [(link(), link()) for _ in range(SP)]
+    def piece(s, dy, dx, h, cut=None):
+        if cut is None:
+            return rows.at[unit(s, dy, dx, h)]
+        return rows.at[unit(s, dy, dx, h), pl.ds(*cut), :]
+
+    def pass_on(s, dy, dx, h, device, cut=None):
+        return send(piece(s, dy, dx, h, cut), piece(s, dy, dx, h, cut), device)
+
+    RQ = RH // 2
+    whole = (0, RH)
+    halves = ((0, RQ), (RQ, RQ))
+    z_units = [
+        (link(), u, cut)
+        for u, cuts in (((0, 0, 0), (whole,)), ((0, 0, 1), (whole,)), ((0, 1, 0), halves), ((1, 0, 1), halves))
+        for cut in cuts
+    ]
+    def links(many):
+        count[0] += many
+        return count[0] - many
+
+    to_mate, to_x, to_y, to_last, to_done = (
+        links(SLOTS), links(SLOTS), links(SLOTS), links(2 * N_CHUNKS), links(3)
+    )
+    ends_of = [k for k in range(N_CHUNKS) if chunk_at(k)[0]]
     common = list(pending)
     pending.clear()
 
     def cols_of(j):
         return pl.ds(pl.multiple_of(j * CB, CB), CB)
 
-    def put(j, h, a, b):
+    def put(j, h, *terms):
         rs = pl.ds(h * RH, RH)
-        out[rs, cols_of(j)] = (mid[rs, cols_of(j)].astype(F32) + a.astype(F32) + b.astype(F32)).astype(BF16)
+        acc = mid[rs, cols_of(j)].astype(F32)
+        for term in terms:
+            acc = acc + term.astype(F32)
+        out[rs, cols_of(j)] = acc.astype(BF16)
+
+    base = count[0]
 
     @pl.when(is_end)
     def _():
         sent = []
 
         def z_unit(i):
-            k, (dy, dx, h) = z_units[i]
-            start(k, piece(1, dy, dx, h), piece(1, dy, dx, h), dev(pz))
+            k, (dy, dx, h), cut = z_units[i]
+            start(k, piece(1, dy, dx, h, cut), piece(1, dy, dx, h, cut), dev(pz))
 
         side_x = pass_on(1, 0, 0, 0, x_dev)
         side_y = pass_on(1, 0, 0, 1, y_dev)
-        cross_up[1].wait_recv()
+        down_first = send(down_half(oy, 0), down_at(z, y, 0), y_dev)
+        z_unit(0)
+        cross_last.wait_recv()
         up_send(z, oy, 1, up_at(z, oy, 1), goal_z, sent)
-        z_unit(0)
         z_unit(1)
-        cross_down.append(
-            send(down_half(oy, 1), down_buf.at[sp, pl.ds(HF, HF), :], y_dev)
-        )
+        down_last = send(down_half(oy, 1), down_at(z, y, 1), y_dev)
         side_x.wait_recv()
         z_unit(2)
+        z_unit(3)
         side_y.wait_recv()
-        z_unit(3)
-        for copy in cross_down:
-            copy.wait_recv()
+        z_unit(4)
+        z_unit(5)
+        down_first.wait_recv()
+        down_last.wait_recv()
         for yy in range(2):
-            down_send(z, yy, down_at(z, yy), goal_z, sent)
-        order = [(zs, yy) for zs in (pz, NZ - 1 - pz, z, NZ - 1 - z) for yy in range(2)]
+            for i in range(2):
+                down_send(z, yy, i, goal_z, sent)
+        order = (pz, NZ - 1 - pz, z, NZ - 1 - z)
         done = []
-        for k, (zs, yy) in enumerate(order):
-            ka, kb = z_parts[k]
-            arrive(ka, z_in.at[k, 0])
-            a = send(z_in.at[k, 0, oy], last_in.at[k, 0], y_dev)
-            arrive(kb, z_in.at[k, 1])
-            b = send(z_in.at[k, 1, ox], last_in.at[k, 1], x_dev)
-            done.append((k, zs * 2 + yy, a, b))
-            if k:
-                end_finish(done[k - 1], z_in, last_in, put, x, y)
+        late = []
+
+        def settle(limit):
+            while late and late[0][0] <= limit:
+                n, m, j = late.pop(0)
+                arrive(to_done + m, z_done.at[m])
+                for h in range(2):
+                    put(j, h, z_done[m, h])
+
+        for k in ends_of:
+            _, n, last = chunk_kind(k)
+            j = order[n // 2] * 2 + n % 2
+            if last:
+                late.append((n, n // 2, j))
+                continue
+            arrive(to_last + 2 * k, z_in.at[n, 0])
+            a = send(z_in.at[n, 0, oy], last_in.at[k, 0], y_dev)
+            arrive(to_last + 2 * k + 1, z_in.at[n, 1])
+            b = send(z_in.at[n, 1, ox], last_in.at[k, 1], x_dev)
+            if done:
+                end_finish(done[-1], z_in, last_in, put, x, y)
+            done.append((k, n, j, a, b))
+            settle(n - 3)
+        settle(SP)
         end_finish(done[-1], z_in, last_in, put, x, y)
         for copy in sent + pending:
             copy.wait_send()
         pending.clear()
-        cross_down.pop()
+
+    count[0] = base
 
     @pl.when(heavy)
     def _():
@@ -662,9 +741,9 @@
             hands[s, dy, dx, h] = pass_on(s, dy, dx, h, mate_dev)
 
         def z_arrive(i):
-            k, (dy, dx, h) = z_units[i]
-            arrive(k, piece(1, dy, dx, h))
-            return pass_on(1, dy, dx, h, x_dev if h else y_dev)
+            k, (dy, dx, h), cut = z_units[i]
+            arrive(k, piece(1, dy, dx, h, cut))
+            return pass_on(1, dy, dx, h, x_dev if h else y_dev, cut)
 
         def up_relay(yy):
             for i in range(2):
@@ -675,210 +754,285 @@
         yb = pass_on(0, 0, 0, 1, y_dev)
         xb = pass_on(0, 0, 0, 1, x_dev)
         ya = pass_on(0, 0, 0, 0, y_dev)
+        down_first = send(down_half(oy, 0), down_at(z, y, 0), y_dev)
         hand(0, 0, 0, 0)
         hand(0, 0, 0, 1)
-        cross_down.append(
-            send(down_half(oy, 1), down_buf.at[sp, pl.ds(HF, HF), :], y_dev)
-        )
+        cross_last.wait_recv()
+        up_send(z, oy, 1, up_at(z, oy, 1), goal_z, sent)
         up_relay(y)
-        cross_up[1].wait_recv()
-        up_send(z, oy, 1, up_at(z, oy, 1), goal_z, sent)
         xa.wait_recv()
-        corner_a = pass_on(0, 0, 1, 0, y_dev)
+        corner_a = [pass_on(0, 0, 1, 0, y_dev, halves[0])]
+        down_last = send(down_half(oy, 1), down_at(z, y, 1), y_dev)
         hand(0, 0, 1, 0)
         yb.wait_recv()
         corner_b = pass_on(0, 1, 0, 1, x_dev)
         hand(0, 1, 0, 1)
-        up_relay(oy)
-        down_send(z, y, down_at(z, y), goal_z, sent)
         ends = {}
         ends[1, 0, 0] = z_arrive(0)
         hand(1, 0, 0, 0)
+        up_relay(oy)
+        down_send(z, y, 0, mz, sent)
+        down_send(z, y, 1, mz, sent)
         xb.wait_recv()
         hand(0, 0, 1, 1)
         ya.wait_recv()
+        corner_a.append(pass_on(0, 1, 0, 0, x_dev, halves[1]))
         hand(0, 1, 0, 0)
-        ends[0, 1, 1] = z_arrive(1)
-        hand(1, 0, 0, 1)
-        for copy in cross_down:
-            copy.wait_recv()
-        down_send(z, oy, down_at(z, oy), goal_z, sent)
-        corner_a.wait_recv()
-        hand(0, 1, 1, 0)
-        corner_b.wait_recv()
-        hand(0, 1, 1, 1)
-        for zs in (mz, NZ - 1 - pz):
+        fz = NZ - 1 - pz
+
+        def up_arrived(zs):
             for yy in range(2):
                 for i in range(2):
                     up_wait(zs, yy, i)
 
-        def up_rows(s, dy, dx):
+        up_arrived(mz)
+
+        KQ = D // NZ
+        near_k = pl.ds(pl.multiple_of(jnp.where(fz == 0, KQ, 0), KQ), D - KQ)
+        far_k = pl.ds(pl.multiple_of(fz * KQ, KQ), KQ)
+
+        def handed(s, group):
+            for dy, dx in group:
+                for h in range(2):
+                    hands[s, dy, dx, h].wait_recv()
+
+        def over(group, one):
+            first = group[0][0] * 2 + group[0][1]
+            lax.fori_loop(first, first + len(group), one, 0)
+
+        def chip(n):
+            return (y + n // 2) % 2 * 2 + (x + n % 2) % 2
+
+        def units_of(i):
+            return pl.ds(pl.multiple_of(i * 4, 4), 4)
+
+        def up_near(group):
+            handed(0, group)
+
+            def one(n, _):
+                i = chip(n)
+                up_sum[i] = dot(rows[units_of(i), :, near_k].reshape(2 * RT, D - KQ), up_buf[near_k, :])
+                return 0
+
+            over(group, one)
+
+        def up_far(group):
+            def one(n, _):
+                i = chip(n)
+                h = up_sum[i] + dot(rows[units_of(i), :, far_k].reshape(2 * RT, KQ), up_buf[far_k, :])
+                h = jnp.maximum(h, 0.0)
+                hidden[i] = (h * h).astype(BF16)
+                return 0
+
+            over(group, one)
+
+        def up_rows(s, group):
+            handed(s, group)
+
+            def one(n, _):
+                i = s * 4 + chip(n)
+                h = jnp.maximum(dot(rows[units_of(i)].reshape(2 * RT, D), up_buf[...]), 0.0)
+                hidden[i] = (h * h).astype(BF16)
+                return 0
+
+            over(group, one)
+
+        slots = SLOTS
+
+        def plane_of(i):
+            if isinstance(i, int):
+                return (z, mz, pz, NZ - 1 - pz)[i]
+            return jnp.where(i == 0, z, jnp.where(i == 1, mz, jnp.where(i == 2, pz, NZ - 1 - pz)))
+
+        def down_ready(i, yy):
+            zs = (z, mz, pz, NZ - 1 - pz)[i]
             for h in range(2):
-                hands[s, dy, dx, h].wait_recv()
-            i = (s * 2 + (y + dy) % 2) * 2 + (x + dx) % 2
-            us = pl.ds(pl.multiple_of(i * 4, 4), 4)
-
-            def one(j, _):
-                cs = pl.ds(pl.multiple_of(j * 512, 512), 512)
-                h = jnp.maximum(dot(rows[us].reshape(2 * RT, D), up_buf[:, cs]), 0.0)
-                hidden[i, :, cs] = (h * h).astype(BF16)
-                return 0
-
-            lax.fori_loop(0, FH // 512, one, 0)
-
-        up_rows(0, 0, 0)
-        ends[1, 1, 0] = z_arrive(2)
-        hand(1, 0, 1, 0)
-        up_rows(0, 0, 1)
-        ends[1, 1, 1] = z_arrive(3)
-        hand(1, 1, 0, 1)
-        up_rows(0, 1, 0)
-        up_rows(0, 1, 1)
-
-        chain = (z, mz, pz, NZ - 1 - pz)
-        chunks = (
-            [(0, 0, yy) for yy in range(2)] + [(0, 1, yy) for yy in range(2)]
-            + [(1, 0, yy) for yy in range(2)] + [(1, 1, yy) for yy in range(2)]
-            + [(s, i, yy) for i in (2, 3) for yy in range(2) for s in range(2)]
-        )
-        waited = set()
-        relays = []
-        slots = part.shape[0]
-        stage = [dict() for _ in chunks]
-        of_set = [sum(1 for t in chunks[:k] if t[0] == chunks[k][0]) for k in range(len(chunks))]
-
-        def down_ready(i, yy):
-            if (i, yy) in waited or i == 0:
-                return
-            waited.add((i, yy))
-            down_wait(chain[i], yy)
-            if i == 2:
-                down_send(pz, yy, down_at(pz, yy), mz, sent)
+                down_wait(zs, yy, h)
+                if i == 2:
+                    relay_of(yy, h).start()
+
+        relay_slots = [[z_slot() for _ in range(2)] for _ in range(2)]
+
+        def relay_of(yy, h):
+            ref = down_at(pz, yy, h)
+            return z_copy(relay_slots[yy][h], down_sem(pz, yy, h), ref, ref, mz)
+
+        def d_mate(k):
+            return copy_of(to_mate + k % slots, part.at[k % slots, :, :, :, 1 - c], mate_in.at[k % slots], mate_dev)
+
+        def d_x(k):
+            return copy_of(to_x + k % slots, part.at[k % slots, :, ox, 0, c], x_in.at[k % slots], x_dev)
+
+        def d_y(k):
+            return copy_of(to_y + k % slots, part.at[k % slots, oy, :, 1, c], y_in.at[k % slots], y_dev)
+
+        def d_last(k, h):
+            src = part.at[k % slots, y, ox, 1, c] if h else part.at[k % slots, oy, x, 0, c]
+            return copy_of(to_last + 2 * k + h, src, last_in.at[k, h], x_dev if h else y_dev)
+
+        def d_through(k, h):
+            src = part.at[k % slots, y, :, 1, c] if h else part.at[k % slots, :, x, 0, c]
+            return copy_of(to_last + 2 * k + h, src, z_in.at[chunk_kind(k)[1], h], dev(pz))
+
+        def d_done(k):
+            m = chunk_kind(k)[1] // 2
+            return copy_of(to_done + m, part.at[k % slots, y, x, :, c], z_done.at[m], dev(pz))
+
+        def split(k, through, other):
+            s, n, last = chunk_kind(k)
+            if isinstance(k, int):
+                (through if s and not last else other)()
+            else:
+                pl.when((s == 1) & jnp.logical_not(last))(through)
+                pl.when((s == 0) | last)(other)
+
+        def sent_all(k):
+            d_mate(k).wait_send()
+            d_x(k).wait_send()
+            d_y(k).wait_send()
+
+            def through():
+                for h in range(2):
+                    d_through(k, h).wait_send()
+
+            def other():
+                for h in range(2):
+                    d_last(k, h).wait_send()
+
+            split(k, through, other)
+
+            @pl.when(chunk_kind(k)[2])
+            def _():
+                d_done(k).wait_send()
 
         def multiply(k):
-            s, i, yy = chunks[k]
-            down_ready(i, yy)
-            if k >= slots:
-                for copy in stage[k - slots]["sent"]:
-                    copy.wait_send()
-            j = chain[i] * 2 + yy
-            slot = k % slots
-
-            def one(q, _):
-                got = dot(hidden[s * 4 + q], down_buf[j]).astype(BF16)
-                part[slot, q // 2, q % 2] = got.reshape(2, 2, RH, CB)
-                return 0
-
-            lax.fori_loop(0, 4, one, 0)
-            mate = copy_of(link(), part.at[slot, :, :, :, 1 - c], mate_in.at[k], mate_dev)
-            mate.start()
-            stage[k]["mate"] = mate
-            stage[k]["sent"] = [mate]
+            s, i, yy = chunk_at(k)
+            j = plane_of(i) * 2 + yy
+            got = dot(hidden[pl.ds(s * 4, 4)].reshape(8 * RT, FH), down_buf[j]).astype(BF16)
+            part[k % slots] = got.reshape(2, 2, 2, 2, RH, CB)
+            d_mate(k).start()
 
         def fold(k):
             slot = k % slots
-            stage[k]["mate"].wait_recv()
+            d_mate(k).wait_recv()
 
             def one(q, _):
                 for h in range(2):
                     part[slot, q // 2, q % 2, h, c] = (
-                        part[slot, q // 2, q % 2, h, c].astype(F32) + mate_in[k, q // 2, q % 2, h].astype(F32)
+                        part[slot, q // 2, q % 2, h, c].astype(F32) + mate_in[slot, q // 2, q % 2, h].astype(F32)
                     ).astype(BF16)
                 return 0
 
             lax.fori_loop(0, 4, one, 0)
-            to_x = copy_of(link(), part.at[slot, :, ox, 0, c], x_in.at[k], x_dev)
-            to_x.start()
-            to_y = copy_of(link(), part.at[slot, oy, :, 1, c], y_in.at[k], y_dev)
-            to_y.start()
-            stage[k]["x"], stage[k]["y"] = to_x, to_y
-            stage[k]["sent"] += [to_x, to_y]
+            d_x(k).start()
+            d_y(k).start()
 
         def spread(k):
             slot = k % slots
-            s = chunks[k][0]
-            stage[k]["x"].wait_recv()
+            d_x(k).wait_recv()
             for i in range(2):
                 part[slot, i, x, 0, c] = (
-                    part[slot, i, x, 0, c].astype(F32) + x_in[k, i].astype(F32)
+                    part[slot, i, x, 0, c].astype(F32) + x_in[slot, i].astype(F32)
                 ).astype(BF16)
-            n = of_set[k]
-            if s:
-                a = copy_of(z_parts[n][0], part.at[slot, :, x, 0, c], z_in.at[n, 0], dev(pz))
-            else:
-                a = copy_of(link(), part.at[slot, oy, x, 0, c], last_in.at[n, 0], y_dev)
-            a.start()
-            stage[k]["y"].wait_recv()
+            split(k, lambda: d_through(k, 0).start(), lambda: d_last(k, 0).start())
+            d_y(k).wait_recv()
             for i in range(2):
                 part[slot, y, i, 1, c] = (
-                    part[slot, y, i, 1, c].astype(F32) + y_in[k, i].astype(F32)
+                    part[slot, y, i, 1, c].astype(F32) + y_in[slot, i].astype(F32)
                 ).astype(BF16)
-            if s:
-                b = copy_of(z_parts[n][1], part.at[slot, y, :, 1, c], z_in.at[n, 1], dev(pz))
-            else:
-                b = copy_of(link(), part.at[slot, y, ox, 1, c], last_in.at[n, 1], x_dev)
-            b.start()
-            stage[k]["last"] = (a, b)
-            stage[k]["sent"] += [a, b]
+            split(k, lambda: d_through(k, 1).start(), lambda: d_last(k, 1).start())
 
         def finish(k):
-            s, i, yy = chunks[k]
-            if s:
-                return
+            s, n, last = chunk_kind(k)
             slot = k % slots
-            n = of_set[k]
-            j = chain[i] * 2 + yy
-            for h, copy in enumerate(stage[k]["last"]):
-                copy.wait_recv()
-                put(j, h, part[slot, y, x, h, c], last_in[n, h])
-
-        reached = [0, 0, 0]
-
-        def advance(which, limit):
-            for k in range(reached[which], max(limit, reached[which])):
-                (fold, spread, finish)[which](k)
-            reached[which] = max(limit, reached[which])
-
-        n_chunks = len(chunks)
-        for k in range(n_chunks):
-            if k == 4:
-                advance(0, k)
-                ends[1, 0, 0].wait_recv()
-                hand(1, 1, 0, 0)
-                ends[0, 1, 1].wait_recv()
-                hand(1, 0, 1, 1)
-                up_rows(1, 0, 0)
-                advance(1, 1)
-                up_rows(1, 0, 1)
-                advance(1, 2)
-                ends[1, 1, 0].wait_recv()
-                hand(1, 1, 1, 0)
-                ends[1, 1, 1].wait_recv()
-                hand(1, 1, 1, 1)
-                up_rows(1, 1, 0)
-                advance(1, 3)
-                up_rows(1, 1, 1)
-                down_ready(2, 0)
-            elif k in (10, 12, 14):
-                advance(0, k)
-                advance(1, k - 1)
-                advance(2, k - 3)
-            else:
-                advance(2, k - 6)
-                advance(1, k - 4)
-                advance(0, k - 2)
-            if k == 7:
-                down_ready(2, 1)
+            j = plane_of(n // 2) * 2 + n % 2
+
+            @pl.when(s == 0)
+            def _():
+                for h in range(2):
+                    d_last(k, h).wait_recv()
+                    put(j, h, part[slot, y, x, h, c], last_in[k, h])
+
+            @pl.when(last)
+            def _():
+                for h in range(2):
+                    d_last(k, h).wait_recv()
+                    part[slot, y, x, h, c] = (
+                        part[slot, y, x, h, c].astype(F32) + last_in[k, h].astype(F32)
+                    ).astype(BF16)
+                d_done(k).start()
+
+        most = ((0, 0), (0, 1), (1, 0))
+        far_corner = ((1, 1),)
+        up_near(most)
+        ends[0, 1, 1] = z_arrive(1)
+        hand(1, 0, 0, 1)
+        down_first.wait_recv()
+        down_send(z, oy, 0, mz, sent)
+        corner_b.wait_recv()
+        hand(0, 1, 1, 1)
+        for copy in corner_a:
+            copy.wait_recv()
+        hand(0, 1, 1, 0)
+        ends[1, 1, 0] = [z_arrive(2), z_arrive(3)]
+        hand(1, 0, 1, 0)
+        up_near(far_corner)
+        up_arrived(fz)
+        up_far(most + far_corner)
+        down_last.wait_recv()
+        down_send(z, oy, 1, mz, sent)
+
+        def lead(k, _):
             multiply(k)
-        for k in range(n_chunks - 2, n_chunks + 1):
-            advance(0, k)
-            advance(1, k - 1)
-            advance(2, k - 3)
-        advance(1, n_chunks)
-        advance(2, n_chunks)
-        for k in range(n_chunks - slots, n_chunks):
-            for copy in stage[k]["sent"]:
-                copy.wait_send()
+            return 0
+
+        ends[1, 1, 1] = [z_arrive(4)]
+        lax.fori_loop(0, 2, lead, 0)
+        up_rows(1, ((0, 0),))
+        ends[1, 1, 1].append(z_arrive(5))
+        hand(1, 1, 0, 1)
+        fold(0)
+        fold(1)
+        ends[0, 1, 1].wait_recv()
+        hand(1, 0, 1, 1)
+        ends[1, 0, 0].wait_recv()
+        hand(1, 1, 0, 0)
+        up_rows(1, ((0, 1), (1, 0)))
+        for copy in ends[1, 1, 1]:
+            copy.wait_recv()
+        hand(1, 1, 1, 1)
+        for copy in ends[1, 1, 0]:
+            copy.wait_recv()
+        hand(1, 1, 1, 0)
+        down_ready(1, 0)
+        down_ready(1, 1)
+        lax.fori_loop(2, 4, lead, 0)
+        down_ready(2, 0)
+        spread(0)
+        up_rows(1, far_corner)
+        fold(2)
+        spread(1)
+
+        def turn(k, _):
+            pl.when(k >= 5)(lambda: finish(k - 5))
+            pl.when((k >= 5) & (k < N_CHUNKS + 3))(lambda: spread(k - 3))
+            pl.when(k < N_CHUNKS + 1)(lambda: fold(k - 1))
+            for at, i, yy in ((6, 2, 1), (12, 3, 0), (13, 3, 1)):
+                pl.when(k == at)(lambda i=i, yy=yy: down_ready(i, yy))
+            pl.when((k >= slots) & (k < N_CHUNKS))(lambda: sent_all(k - slots))
+            pl.when(k < N_CHUNKS)(lambda: multiply(k))
+            return 0
+
+        lax.fori_loop(OWN_LEAD, N_CHUNKS + 5, turn, 0)
+
+        def drain(k, _):
+            sent_all(k)
+            return 0
+
+        lax.fori_loop(N_CHUNKS - slots, N_CHUNKS, drain, 0)
+        for yy in range(2):
+            for h in range(2):
+                relay_of(yy, h).wait_send()
         for copy in sent + pending:
             copy.wait_send()
         pending.clear()
@@ -892,11 +1046,11 @@
 
 
 def end_finish(one, z_in, last_in, put, x, y):
-    k, j, a, b = one
+    k, n, j, a, b = one
     a.wait_recv()
-    put(j, 0, z_in[k, 0, y], last_in[k, 0])
+    put(j, 0, z_in[n, 0, y], last_in[k, 0])
     b.wait_recv()
-    put(j, 1, z_in[k, 1, x], last_in[k, 1])
+    put(j, 1, z_in[n, 1, x], last_in[k, 1])
 
 
 def one_kernel(SP, TP, *args):
@@ -908,17 +1062,14 @@
     RH = RT // 2
     FH = up.shape[1] // 2
     CB = down.shape[1]
-    heads = dw.shape[0] + dn.shape[0]
-    decay = jnp.concatenate([dw, dn]).reshape(heads * NB, BLOCK)
-    decay = jnp.pad(decay, ((0, 128 - heads * NB), (0, 0)))
     offs, starts = turn_tables(SP, T)
     vmem = pl.BlockSpec(memory_space=pltpu.VMEM)
     hbm = pl.BlockSpec(memory_space=pl.ANY)
-    copies = 256
+    copies = 118
     return pl.pallas_call(
         functools.partial(layer_kernel, SP, TP),
         out_shape=jax.ShapeDtypeStruct((RT, D), BF16),
-        in_specs=[vmem] * 13 + [hbm] * 4,
+        in_specs=[vmem] * 14 + [hbm] * 4,
         out_specs=vmem,
         scratch_shapes=[
             pltpu.VMEM((D, FH), BF16),
@@ -933,24 +1084,27 @@
             pltpu.VMEM((RT, D), BF16),
             pltpu.VMEM((32, RH, D), BF16),
             pltpu.VMEM((8, 2 * RT, FH), BF16),
-            pltpu.VMEM((8, 2, 2, 2, 2, RH, CB), BF16),
-            pltpu.VMEM((2 * SP, 2, 2, 2, RH, CB), BF16),
+            pltpu.VMEM((SLOTS, 2, 2, 2, 2, RH, CB), BF16),
+            pltpu.VMEM((SLOTS, 2, 2, 2, RH, CB), BF16),
+            pltpu.VMEM((SLOTS, 2, RH, CB), BF16),
+            pltpu.VMEM((SLOTS, 2, RH, CB), BF16),
             pltpu.VMEM((2 * SP, 2, RH, CB), BF16),
-            pltpu.VMEM((2 * SP, 2, RH, CB), BF16),
-            pltpu.VMEM((SP, 2, RH, CB), BF16),
             pltpu.VMEM((SP, 2, 2, RH, CB), BF16),
+            pltpu.VMEM((3, 2, RH, CB), BF16),
+            pltpu.VMEM((128, 128), F32),
+            pltpu.VMEM((4, 2 * RT, FH), F32),
             pltpu.SemaphoreType.DMA((copies,)),
             pltpu.SemaphoreType.DMA((copies,)),
-            pltpu.SemaphoreType.DMA((8,)),
-            pltpu.SemaphoreType.DMA((24,)),
-            pltpu.SemaphoreType.DMA((24,)),
+            pltpu.SemaphoreType.DMA((6,)),
+            pltpu.SemaphoreType.DMA((22,)),
+            pltpu.SemaphoreType.DMA((32,)),
             pltpu.SemaphoreType.DMA((4,)),
         ],
         compiler_params=pltpu.CompilerParams(
             collective_id=0, has_side_effects=True, vmem_limit_bytes=63 * 1024 * 1024
         ),
-    )(stream, qw, kw, vw, gw, qn, kn, vn, gn, decay, jnp.asarray(offs), jnp.asarray(starts),
-      gain.reshape(1, D), ow, on, up, down)
+    )(stream, qw, kw, vw, gw, qn, kn, vn, gn, dw, dn, jnp.asarray(offs), jnp.asarray(starts),
+      gain, ow, on, up, down)
 
 
 def fits_kernel(SP, TP, args):

time: 161 us -> 140 us (0.87)
  Pallas kernels: 156 us -> 138 us
  local copies, waits for them, and re-layouts: 4.06 us -> 2.09 us
    pallas_call x1, Pallas kernels: 156 us -> 138 us  [one_kernel(): pl.pallas_call(functools.partial(layer_kernel, SP, TP), out_shape=jax.Sha...]
where the time goes in v2:
time: 140 us
  Pallas kernels  138 us (99%)
  local copies, waits for them, and re-layouts  2.09 us (1%)
    pallas_call x1, Pallas kernels, one_kernel(): pl.pallas_call(functools.partial(layer_kernel, SP, TP), out_shape=jax.Sha...  138 us

profile of v2, /device:TPU:0, one launch (start us, length us, event | category | flops | bytes accessed | tf_op | source)
XLA Modules:
  0.0 140.0 jit_solution(4598769393439114372)
XLA Ops:
  0.0 137.9 %shard_map.172 = bf16[192,2048]{1,0:T(8,128)(2,1)} custom-call(bf16[192,2048]{1,0:T(8,128)(2,1)} %stream.1, bf16[768,128]{1,0:T(8,128)(2,1)} %qw.1, bf16[768,128]{1,0:T(8,128)(2,1)} %kw.1, bf16[768,128]{1,0:T(8,128)(2,1)} %vw.1, bf16[768,128]{1,0:T(8,128)(2,1)} %gw.1, bf16[768,128]{1,0:T(8,128)(2,1)} %qn.1, bf16[768,128]{1,0:T(8,128)(2,1)} %kn.1, ...), custom_call_target="tpu_custom_call" | custom-call | tf_op jit(solution)/shard_map/pallas_call | solution.py:1069
  137.9 2.1 %copy.20 = bf16[192,2048]{1,0:T(8,128)(2,1)} copy(bf16[192,2048]{1,0:T(8,128)(2,1)} %shard_map.172) | data formatting | bytes 1572864

commit v3 on v2

--- a/solution.py
+++ b/solution.py
@@ -250,30 +250,30 @@
 def chunk_kind(k):
     s, i, yy = chunk_at(k)
     n = i * 2 + yy
-    last = (s == 1) & (yy == 1) & (i < 3)
+    last = (s == 1) & (yy == 1) & (i > 0)
     return s, n, last
 
 
 def layer_kernel(
     SP, TP,
-    stream, qw, kw, vw, gw, qn, kn, vn, gn, dw, dn, offs, starts, gain, ow_w, ow_n, up, down,
-    out,
+    kw, vw, kn, vn, dw, dn, offs, starts, gain, stream_at, qw_at, qn_at, gw_at, gn_at, ow_w, ow_n, up, down,
+    out_at,
     up_buf, down_buf, ow_buf, st_buf, k_rot, before, inside, mixed, mix_in, mid, rows, hidden, part,
-    mate_in, x_in, y_in, last_in, z_in, z_done, rates_buf, up_sum,
-    ssem, rsem, lsem, zsend, zrecv, srecv,
+    mate_in, x_in, y_in, last_in, z_in, z_done, rates_buf, up_sum, stream, qw, qn, gw, gn, out,
+    ssem, rsem, lsem, zsend, zrecv, srecv, osem,
 ):
     sp = lax.axis_index("sp")
     tp = lax.axis_index("tp")
     NZ = SP // 2
     z, y = sp // 2, sp % 2
     x, c = tp // 2, tp % 2
-    T = qw.shape[0]
+    T = kw.shape[0]
     NB = T // BLOCK
     RT = T // TP
     RH = RT // 2
     RB = up.shape[0]
     CB = down.shape[1]
-    D = stream.shape[1]
+    D = up_buf.shape[0]
     FH = up.shape[1] // 2
     heavy = (z == 1) | (z == 2)
     is_end = jnp.logical_not(heavy)
@@ -292,9 +292,9 @@
         count[0] += 1
         return count[0] - 1
 
-    def copy_of(k, src, dst, device):
+    def copy_of(k, src, dst, device, ks=None):
         return pltpu.make_async_remote_copy(
-            src_ref=src, dst_ref=dst, send_sem=ssem.at[k], recv_sem=rsem.at[k],
+            src_ref=src, dst_ref=dst, send_sem=ssem.at[k if ks is None else ks], recv_sem=rsem.at[k],
             device_id=device, device_id_type=MESH_ID,
         )
 
@@ -310,20 +310,22 @@
     def arrive(k, dst):
         copy_of(k, dst, dst, mate_dev).wait_recv()
 
+    locals_ = []
+
+    def keep(src, dst):
+        copy = pltpu.make_async_copy(src, dst, lsem.at[len(locals_)])
+        copy.start()
+        locals_.append(copy)
+        return copy
+
     barrier = pltpu.get_barrier_semaphore()
     for d in range(1, NZ):
         pl.semaphore_signal(barrier, inc=1, device_id=dev((z + d) % NZ), device_id_type=MESH_ID)
     for device in (x_dev, y_dev, mate_dev, dev(z, 0, 1, 1)):
         pl.semaphore_signal(barrier, inc=1, device_id=device, device_id_type=MESH_ID)
+    for src, dst in ((qw_at, qw), (qn_at, qn), (gw_at, gw), (gn_at, gn), (stream_at, stream)):
+        keep(src, dst)
     pl.semaphore_wait(barrier, NZ + 3)
-
-    locals_ = []
-
-    def keep(src, dst):
-        copy = pltpu.make_async_copy(src, dst, lsem.at[len(locals_)])
-        copy.start()
-        locals_.append(copy)
-        return copy
 
     HB = RB // 2
     HF = FH // 2
@@ -490,6 +492,8 @@
     state_y = send(st_buf.at[0], st_buf.at[1], y_dev)
     cross_first.append(cross_rows(QB, HB - QB))
 
+    for copy in locals_[:2]:
+        copy.wait()
     for b in range(NB):
         rs = pl.ds(b * BLOCK, BLOCK)
         kwr, knr = k_rot[rs, 0:128], k_rot[rs, 128:256]
@@ -565,6 +569,8 @@
     s_w = held[0]
     s_n = jnp.concatenate([jnp.where(low_half, held[1], 0.0), jnp.where(low_half, 0.0, held[1])], axis=0)
 
+    for copy in locals_[2:4]:
+        copy.wait()
     sums = [jnp.zeros((1, 1), F32) for _ in range(3)]
     for b in range(NB):
         rs = pl.ds(b * BLOCK, BLOCK)
@@ -602,7 +608,7 @@
     ow_hand.append(send(ow_buf.at[side, :, relay_cols(oy)], ow_buf.at[side, :, relay_cols(oy)], mate_dev))
     for copy in ow_mate + ow_hand + swaps:
         copy.wait_recv()
-    for copy in locals_:
+    for copy in locals_[4:]:
         copy.wait()
 
     def project(i, _):
@@ -644,6 +650,7 @@
     RQ = RH // 2
     whole = (0, RH)
     halves = ((0, RQ), (RQ, RQ))
+    thirds = ((0, RH // 3), (RH // 3, RH - RH // 3))
     z_units = [
         (link(), u, cut)
         for u, cuts in (((0, 0, 0), (whole,)), ((0, 0, 1), (whole,)), ((0, 1, 0), halves), ((1, 0, 1), halves))
@@ -654,7 +661,7 @@
         return count[0] - many
 
     to_mate, to_x, to_y, to_last, to_done = (
-        links(SLOTS), links(SLOTS), links(SLOTS), links(2 * N_CHUNKS), links(3)
+        links(SLOTS), links(SLOTS), links(SLOTS), links(2 * SLOTS), links(3)
     )
     ends_of = [k for k in range(N_CHUNKS) if chunk_at(k)[0]]
     common = list(pending)
@@ -671,6 +678,9 @@
         out[rs, cols_of(j)] = acc.astype(BF16)
 
     base = count[0]
+
+    def put_out(j):
+        pltpu.make_async_copy(out.at[:, cols_of(j)], out_at.at[:, cols_of(j)], osem).start()
 
     @pl.when(is_end)
     def _():
@@ -709,23 +719,24 @@
                 arrive(to_done + m, z_done.at[m])
                 for h in range(2):
                     put(j, h, z_done[m, h])
+                put_out(j)
 
         for k in ends_of:
             _, n, last = chunk_kind(k)
             j = order[n // 2] * 2 + n % 2
             if last:
-                late.append((n, n // 2, j))
+                late.append((n, n // 2 - 1, j))
                 continue
-            arrive(to_last + 2 * k, z_in.at[n, 0])
+            arrive(to_last + 2 * n, z_in.at[n, 0])
             a = send(z_in.at[n, 0, oy], last_in.at[k, 0], y_dev)
-            arrive(to_last + 2 * k + 1, z_in.at[n, 1])
+            arrive(to_last + 2 * n + 1, z_in.at[n, 1])
             b = send(z_in.at[n, 1, ox], last_in.at[k, 1], x_dev)
             if done:
-                end_finish(done[-1], z_in, last_in, put, x, y)
+                end_finish(done[-1], z_in, last_in, put, put_out, x, y)
             done.append((k, n, j, a, b))
             settle(n - 3)
         settle(SP)
-        end_finish(done[-1], z_in, last_in, put, x, y)
+        end_finish(done[-1], z_in, last_in, put, put_out, x, y)
         for copy in sent + pending:
             copy.wait_send()
         pending.clear()
@@ -735,10 +746,12 @@
     @pl.when(heavy)
     def _():
         sent = []
-        hands = {}
+        hand_send = link()
+        hand_first = links(8)
 
         def hand(s, dy, dx, h):
-            hands[s, dy, dx, h] = pass_on(s, dy, dx, h, mate_dev)
+            ref = piece(s, dy, dx, h)
+            copy_of(hand_first + (s * 2 + dy) * 2 + dx, ref, ref, mate_dev, hand_send).start()
 
         def z_arrive(i):
             k, (dy, dx, h), cut = z_units[i]
@@ -761,7 +774,7 @@
         up_send(z, oy, 1, up_at(z, oy, 1), goal_z, sent)
         up_relay(y)
         xa.wait_recv()
-        corner_a = [pass_on(0, 0, 1, 0, y_dev, halves[0])]
+        corner_a = [pass_on(0, 0, 1, 0, y_dev, thirds[0])]
         down_last = send(down_half(oy, 1), down_at(z, y, 1), y_dev)
         hand(0, 0, 1, 0)
         yb.wait_recv()
@@ -776,7 +789,7 @@
         xb.wait_recv()
         hand(0, 0, 1, 1)
         ya.wait_recv()
-        corner_a.append(pass_on(0, 1, 0, 0, x_dev, halves[1]))
+        corner_a.append(pass_on(0, 1, 0, 0, x_dev, thirds[1]))
         hand(0, 1, 0, 0)
         fz = NZ - 1 - pz
 
@@ -793,8 +806,7 @@
 
         def handed(s, group):
             for dy, dx in group:
-                for h in range(2):
-                    hands[s, dy, dx, h].wait_recv()
+                arrive(hand_first + (s * 2 + dy) * 2 + dx, rows.at[pl.ds(0, 2)])
 
         def over(group, one):
             first = group[0][0] * 2 + group[0][1]
@@ -868,14 +880,15 @@
 
         def d_last(k, h):
             src = part.at[k % slots, y, ox, 1, c] if h else part.at[k % slots, oy, x, 0, c]
-            return copy_of(to_last + 2 * k + h, src, last_in.at[k, h], x_dev if h else y_dev)
+            return copy_of(to_last + 2 * (k % slots) + h, src, last_in.at[k, h], x_dev if h else y_dev)
 
         def d_through(k, h):
             src = part.at[k % slots, y, :, 1, c] if h else part.at[k % slots, :, x, 0, c]
-            return copy_of(to_last + 2 * k + h, src, z_in.at[chunk_kind(k)[1], h], dev(pz))
+            n = chunk_kind(k)[1]
+            return copy_of(to_last + 2 * n + h, src, z_in.at[n, h], dev(pz), to_last + 2 * (k % slots) + h)
 
         def d_done(k):
-            m = chunk_kind(k)[1] // 2
+            m = chunk_kind(k)[1] // 2 - 1
             return copy_of(to_done + m, part.at[k % slots, y, x, :, c], z_done.at[m], dev(pz))
 
         def split(k, through, other):
@@ -952,6 +965,7 @@
                 for h in range(2):
                     d_last(k, h).wait_recv()
                     put(j, h, part[slot, y, x, h, c], last_in[k, h])
+                put_out(j)
 
             @pl.when(last)
             def _():
@@ -1033,6 +1047,7 @@
         for yy in range(2):
             for h in range(2):
                 relay_of(yy, h).wait_send()
+        copy_of(0, rows.at[pl.ds(0, 16)], rows.at[pl.ds(0, 16)], mate_dev, hand_send).wait_send()
         for copy in sent + pending:
             copy.wait_send()
         pending.clear()
@@ -1043,14 +1058,16 @@
             copy.wait_send()
     for copy in common + z_copies:
         copy.wait_send()
-
-
-def end_finish(one, z_in, last_in, put, x, y):
+    pltpu.make_async_copy(out, out_at, osem).wait()
+
+
+def end_finish(one, z_in, last_in, put, put_out, x, y):
     k, n, j, a, b = one
     a.wait_recv()
     put(j, 0, z_in[n, 0, y], last_in[k, 0])
     b.wait_recv()
     put(j, 1, z_in[n, 1, x], last_in[k, 1])
+    put_out(j)
 
 
 def one_kernel(SP, TP, *args):
@@ -1065,12 +1082,13 @@
     offs, starts = turn_tables(SP, T)
     vmem = pl.BlockSpec(memory_space=pltpu.VMEM)
     hbm = pl.BlockSpec(memory_space=pl.ANY)
-    copies = 118
+    heads = qw.shape[1]
+    copies = 94
     return pl.pallas_call(
         functools.partial(layer_kernel, SP, TP),
         out_shape=jax.ShapeDtypeStruct((RT, D), BF16),
-        in_specs=[vmem] * 14 + [hbm] * 4,
-        out_specs=vmem,
+        in_specs=[vmem] * 9 + [hbm] * 9,
+        out_specs=hbm,
         scratch_shapes=[
             pltpu.VMEM((D, FH), BF16),
             pltpu.VMEM((SP, FH, CB), BF16),
@@ -1093,18 +1111,25 @@
             pltpu.VMEM((3, 2, RH, CB), BF16),
             pltpu.VMEM((128, 128), F32),
             pltpu.VMEM((4, 2 * RT, FH), F32),
+            pltpu.VMEM((RT, D), BF16),
+            pltpu.VMEM((T, heads), BF16),
+            pltpu.VMEM((T, heads), BF16),
+            pltpu.VMEM((T, heads), BF16),
+            pltpu.VMEM((T, heads), BF16),
+            pltpu.VMEM((RT, D), BF16),
             pltpu.SemaphoreType.DMA((copies,)),
             pltpu.SemaphoreType.DMA((copies,)),
-            pltpu.SemaphoreType.DMA((6,)),
+            pltpu.SemaphoreType.DMA((11,)),
             pltpu.SemaphoreType.DMA((22,)),
             pltpu.SemaphoreType.DMA((32,)),
             pltpu.SemaphoreType.DMA((4,)),
+            pltpu.SemaphoreType.DMA,
         ],
         compiler_params=pltpu.CompilerParams(
             collective_id=0, has_side_effects=True, vmem_limit_bytes=63 * 1024 * 1024
         ),
-    )(stream, qw, kw, vw, gw, qn, kn, vn, gn, dw, dn, jnp.asarray(offs), jnp.asarray(starts),
-      gain, ow, on, up, down)
+    )(kw, vw, kn, vn, dw, dn, jnp.asarray(offs), jnp.asarray(starts), gain,
+      stream, qw, qn, gw, gn, ow, on, up, down)
 
 
 def fits_kernel(SP, TP, args):

time: 140 us -> 133 us (0.950)
  Pallas kernels: 138 us -> 131 us
    pallas_call x1, Pallas kernels: 138 us -> 131 us  [one_kernel(): pl.pallas_call(functools.partial(layer_kernel, SP, TP), out_shape=jax.Sha...]
where the time goes in v3:
time: 133 us
  Pallas kernels  131 us (98%)
  local copies, waits for them, and re-layouts  2.09 us (2%)
    pallas_call x1, Pallas kernels, one_kernel(): pl.pallas_call(functools.partial(layer_kernel, SP, TP), out_shape=jax.Sha...  131 us

profile of v3, /device:TPU:0, one launch (start us, length us, event | category | flops | bytes accessed | tf_op | source)
XLA Modules:
  0.0 133.2 jit_solution(4265685005301175743)
XLA Ops:
  0.0 131.1 %shard_map.172 = bf16[192,2048]{1,0:T(8,128)(2,1)} custom-call(bf16[768,128]{1,0:T(8,128)(2,1)} %kw.1, bf16[768,128]{1,0:T(8,128)(2,1)} %vw.1, bf16[768,128]{1,0:T(8,128)(2,1)} %kn.1, bf16[768,128]{1,0:T(8,128)(2,1)} %vn.1, f32[1,768]{1,0:T(1,128)} %dw.1, f32[2,768]{1,0:T(2,128)} %dn.1, f32[4,128,128]{2,1,0:T(8,128)} %constant.4.clone.offs, ...), custom_call_target="tpu_custom_call" | custom-call | tf_op jit(solution)/shard_map/pallas_call | solution.py:1087
  131.1 2.1 %copy.20 = bf16[192,2048]{1,0:T(8,128)(2,1)} copy(bf16[192,2048]{1,0:T(8,128)(2,1)} %shard_map.172) | data formatting | bytes 1572864

commit v4 on v3

--- a/solution.py
+++ b/solution.py
@@ -229,29 +229,27 @@
 
 
 N_CHUNKS = 16
-OWN_LEAD = 4
+LEAD = 2
 SLOTS = 8
 
 
+ORDER = [0, 1, 8, 9, 2, 10, 11, 12, 13, 3, 14, 4, 5, 15, 6, 7]
+
+
 def chunk_at(k):
-    t = k - OWN_LEAD
     if isinstance(k, int):
-        if t < 0:
-            return 0, k // 2, k % 2
-        far = t % 3 != 2 if t < 8 else t < 10
-        n = (t - t // 3 if far else 4 + t // 3) if t < 8 else (t - 2 if far else t - 4)
-        return int(far), n // 2, n % 2
-    far = jnp.where(t < 8, jnp.where(t % 3 != 2, 1, 0), jnp.where(t < 10, 1, 0)) == 1
-    early = jnp.where(far, t - t // 3, 4 + t // 3)
-    n = jnp.where(t < 0, k, jnp.where(t < 8, early, jnp.where(far, t - 2, t - 4)))
-    return jnp.where((t >= 0) & far, 1, 0), n // 2, n % 2
+        code = ORDER[k]
+    else:
+        code = ORDER[0]
+        for i, value in enumerate(ORDER[1:], 1):
+            code = jnp.where(k == i, value, code)
+    n = code % 8
+    return code // 8, n // 2, n % 2
 
 
 def chunk_kind(k):
     s, i, yy = chunk_at(k)
-    n = i * 2 + yy
-    last = (s == 1) & (yy == 1) & (i > 0)
-    return s, n, last
+    return s, i * 2 + yy
 
 
 def layer_kernel(
@@ -660,9 +658,8 @@
         count[0] += many
         return count[0] - many
 
-    to_mate, to_x, to_y, to_last, to_done = (
-        links(SLOTS), links(SLOTS), links(SLOTS), links(2 * SLOTS), links(3)
-    )
+    to_mate, to_x, to_y, to_last, to_done = links(SLOTS), links(SLOTS), links(SLOTS), links(2 * SLOTS), link()
+    n_done = 3
     ends_of = [k for k in range(N_CHUNKS) if chunk_at(k)[0]]
     common = list(pending)
     pending.clear()
@@ -711,21 +708,10 @@
                 down_send(z, yy, i, goal_z, sent)
         order = (pz, NZ - 1 - pz, z, NZ - 1 - z)
         done = []
-        late = []
-
-        def settle(limit):
-            while late and late[0][0] <= limit:
-                n, m, j = late.pop(0)
-                arrive(to_done + m, z_done.at[m])
-                for h in range(2):
-                    put(j, h, z_done[m, h])
-                put_out(j)
-
         for k in ends_of:
-            _, n, last = chunk_kind(k)
+            _, n = chunk_kind(k)
             j = order[n // 2] * 2 + n % 2
-            if last:
-                late.append((n, n // 2 - 1, j))
+            if n == n_done:
                 continue
             arrive(to_last + 2 * n, z_in.at[n, 0])
             a = send(z_in.at[n, 0, oy], last_in.at[k, 0], y_dev)
@@ -734,8 +720,11 @@
             if done:
                 end_finish(done[-1], z_in, last_in, put, put_out, x, y)
             done.append((k, n, j, a, b))
-            settle(n - 3)
-        settle(SP)
+        j = order[n_done // 2] * 2 + n_done % 2
+        arrive(to_done, z_done)
+        for h in range(2):
+            put(j, h, z_done[h])
+        put_out(j)
         end_finish(done[-1], z_in, last_in, put, put_out, x, y)
         for copy in sent + pending:
             copy.wait_send()
@@ -888,16 +877,15 @@
             return copy_of(to_last + 2 * n + h, src, z_in.at[n, h], dev(pz), to_last + 2 * (k % slots) + h)
 
         def d_done(k):
-            m = chunk_kind(k)[1] // 2 - 1
-            return copy_of(to_done + m, part.at[k % slots, y, x, :, c], z_done.at[m], dev(pz))
+            return copy_of(to_done, part.at[k % slots, y, x, :, c], z_done, dev(pz))
 
         def split(k, through, other):
-            s, n, last = chunk_kind(k)
+            s, n = chunk_kind(k)
             if isinstance(k, int):
-                (through if s and not last else other)()
+                (through if s and n != n_done else other)()
             else:
-                pl.when((s == 1) & jnp.logical_not(last))(through)
-                pl.when((s == 0) | last)(other)
+                pl.when((s == 1) & (n != n_done))(through)
+                pl.when((s == 0) | (n == n_done))(other)
 
         def sent_all(k):
             d_mate(k).wait_send()
@@ -913,8 +901,9 @@
                     d_last(k, h).wait_send()
 
             split(k, through, other)
-
-            @pl.when(chunk_kind(k)[2])
+            s, n = chunk_kind(k)
+
+            @pl.when((s == 1) & (n == n_done))
             def _():
                 d_done(k).wait_send()
 
@@ -956,7 +945,7 @@
             split(k, lambda: d_through(k, 1).start(), lambda: d_last(k, 1).start())
 
         def finish(k):
-            s, n, last = chunk_kind(k)
+            s, n = chunk_kind(k)
             slot = k % slots
             j = plane_of(n // 2) * 2 + n % 2
 
@@ -967,7 +956,7 @@
                     put(j, h, part[slot, y, x, h, c], last_in[k, h])
                 put_out(j)
 
-            @pl.when(last)
+            @pl.when((s == 1) & (n == n_done))
             def _():
                 for h in range(2):
                     d_last(k, h).wait_recv()
@@ -1018,26 +1007,21 @@
         for copy in ends[1, 1, 0]:
             copy.wait_recv()
         hand(1, 1, 1, 0)
-        down_ready(1, 0)
-        down_ready(1, 1)
-        lax.fori_loop(2, 4, lead, 0)
-        down_ready(2, 0)
+        up_rows(1, far_corner)
         spread(0)
-        up_rows(1, far_corner)
-        fold(2)
-        spread(1)
 
         def turn(k, _):
             pl.when(k >= 5)(lambda: finish(k - 5))
-            pl.when((k >= 5) & (k < N_CHUNKS + 3))(lambda: spread(k - 3))
-            pl.when(k < N_CHUNKS + 1)(lambda: fold(k - 1))
-            for at, i, yy in ((6, 2, 1), (12, 3, 0), (13, 3, 1)):
+            pl.when(k == N_CHUNKS)(lambda: fold(k - 1))
+            for at, i, yy in ((3, 2, 0), (4, 1, 0), (4, 1, 1), (8, 2, 1), (10, 3, 0), (13, 3, 1)):
                 pl.when(k == at)(lambda i=i, yy=yy: down_ready(i, yy))
             pl.when((k >= slots) & (k < N_CHUNKS))(lambda: sent_all(k - slots))
             pl.when(k < N_CHUNKS)(lambda: multiply(k))
+            pl.when((k >= 4) & (k < N_CHUNKS + 3))(lambda: spread(k - 3))
+            pl.when((k > LEAD) & (k < N_CHUNKS))(lambda: fold(k - 1))
             return 0
 
-        lax.fori_loop(OWN_LEAD, N_CHUNKS + 5, turn, 0)
+        lax.fori_loop(LEAD, N_CHUNKS + 5, turn, 0)
 
         def drain(k, _):
             sent_all(k)
@@ -1083,7 +1067,7 @@
     vmem = pl.BlockSpec(memory_space=pltpu.VMEM)
     hbm = pl.BlockSpec(memory_space=pl.ANY)
     heads = qw.shape[1]
-    copies = 94
+    copies = 92
     return pl.pallas_call(
         functools.partial(layer_kernel, SP, TP),
         out_shape=jax.ShapeDtypeStruct((RT, D), BF16),
@@ -1108,7 +1092,7 @@
             pltpu.VMEM((SLOTS, 2, RH, CB), BF16),
             pltpu.VMEM((2 * SP, 2, RH, CB), BF16),
             pltpu.VMEM((SP, 2, 2, RH, CB), BF16),
-            pltpu.VMEM((3, 2, RH, CB), BF16),
+            pltpu.VMEM((2, RH, CB), BF16),
             pltpu.VMEM((128, 128), F32),
             pltpu.VMEM((4, 2 * RT, FH), F32),
             pltpu.VMEM((RT, D), BF16),

time: 133 us -> 133 us (level)
  no operation moved by 1% of the time
where the time goes in v4:
time: 133 us
  Pallas kernels  131 us (98%)
  local copies, waits for them, and re-layouts  2.09 us (2%)
    pallas_call x1, Pallas kernels, one_kernel(): pl.pallas_call(functools.partial(layer_kernel, SP, TP), out_shape=jax.Sha...  131 us

profile of v4, /device:TPU:0, one launch (start us, length us, event | category | flops | bytes accessed | tf_op | source)
XLA Modules:
  0.0 132.7 jit_solution(13920749852604796729)
XLA Ops:
  0.0 130.6 %shard_map.172 = bf16[192,2048]{1,0:T(8,128)(2,1)} custom-call(bf16[768,128]{1,0:T(8,128)(2,1)} %kw.1, bf16[768,128]{1,0:T(8,128)(2,1)} %vw.1, bf16[768,128]{1,0:T(8,128)(2,1)} %kn.1, bf16[768,128]{1,0:T(8,128)(2,1)} %vn.1, f32[1,768]{1,0:T(1,128)} %dw.1, f32[2,768]{1,0:T(2,128)} %dn.1, f32[4,128,128]{2,1,0:T(8,128)} %constant.4.clone.offs, ...), custom_call_target="tpu_custom_call" | custom-call | tf_op jit(solution)/shard_map/pallas_call | solution.py:1071
  130.6 2.1 %copy.20 = bf16[192,2048]{1,0:T(8,128)(2,1)} copy(bf16[192,2048]{1,0:T(8,128)(2,1)} %shard_map.172) | data formatting | bytes 1572864
